TPU v7x, 256 devices: a whole 4x4x8 slice. The times are simulated.
256 devices in a mesh: sp: 32 (over z, x), tp: 8 (over y, core).
Axes of the slice: x: 4, y: 4, z: 8, core: 2. Of those that a mesh axis runs over, the one named last changes fastest.
Arguments:
- activations: bfloat16 [16384, 1024], P(('sp', 'tp')), may hold values from -8 to 8, as said below
- input_gain: float32 [1024], replicated, may hold values from 0.5 to 1.5
- query_weight: bfloat16 [1024, 1024], P(None, 'tp'), may hold values from -0.1875 to 0.1875
- key_weight: bfloat16 [1024, 1024], P(None, 'tp'), may hold values from -0.375 to 0.375
- value_weight: bfloat16 [1024, 1024], P(None, 'tp'), may hold values from -0.1875 to 0.1875
- stop_offset: float32 [16], P('tp'), may hold values from -16 to 0, as said below
- output_weight: bfloat16 [1024, 1024], P('tp'), may hold values from -0.1875 to 0.1875
- output_gain: float32 [1024], replicated, may hold values from 0.5 to 1.5
Outputs:
- layer_out: bfloat16 [16384, 1024], P(('sp', 'tp'))
Inputs may be any that keep to these rules, and one draw needn't show every extreme that they name: activations are noise of about unit size plus a mean vector of about unit size shared by each aligned block of 512 rows and different between runs; each row as a whole may also be scaled by a factor between 0.25 and 2; the result is clipped to the range. `stop_offset`: each entry equals minus the natural logarithm of 16384, minus 2, plus the natural logarithm of 3, plus a number between 0 and 0.7.
All inputs are finite; a program needn't handle non-finite values.
Results may differ from a plain program's by a relative error of at most 0.015.
Values may be sent and summed in bfloat16 or wider, within the bound.
A program may use at most 128 MiB of HBM per device.

v0:
```python
import functools

import jax
import jax.numpy as jnp
from jax import lax
from jax.experimental import pallas as pl
from jax.experimental.pallas import tpu as pltpu
from jax.sharding import PartitionSpec as P

epsilon = 1e-06
log2e = 1.4426950408889634
MESH = pl.DeviceIdType.MESH
f32 = jnp.float32
bf16 = jnp.bfloat16


def scaled_rows(widened, row_gain):
    spread = jnp.mean(widened * widened, axis=-1, keepdims=True)
    return (widened * lax.rsqrt(spread + epsilon) * row_gain).astype(bf16)


def layer_kernel(
    S,
    T,
    H,
    dh,
    act,
    gain_in,
    wq_hbm,
    wk_hbm,
    wv_hbm,
    off,
    wo_hbm,
    gain_out,
    out,
    wq,
    wk,
    wv,
    xg,
    wg,
    kvs,
    qs,
    kv,
    qr,
    qpad,
    tri,
    acc,
    carry,
    obuf,
    orecv,
    att,
    x_send,
    x_recv,
    w_send,
    w_recv,
    kv_send,
    kv_relay,
    kv_recv,
    q_send,
    q_recv,
    o_send,
    o_recv,
    load,
):
    G = S // H
    R = act.shape[0]
    B = R * T
    half = B // 2
    rows = wo_hbm.shape[0]
    s = lax.axis_index("sp")
    t = lax.axis_index("tp")
    h, g = s // G, s % G
    y, c = t // 2, t % 2
    partner = y * 2 + 1 - c
    Y = T // 2

    def owner(group):
        turn = s % (2 * G) if group is None else None
        return jnp.where(turn < G, turn, 2 * G - 1 - turn)

    gq = owner(None)

    def block_of(k):
        return k * G + (g if k % 2 == 0 else G - 1 - g)

    def remote(src, dst, send, recv, dev):
        return pltpu.make_async_remote_copy(
            src_ref=src, dst_ref=dst, send_sem=send, recv_sem=recv, device_id=dev, device_id_type=MESH
        )

    started = []

    def go(copy):
        copy.start()
        started.append(copy)
        return copy

    def xrow(index):
        return xg.at[pl.ds(pl.multiple_of(index * R, R), R)]

    def wrow(index):
        return wg.at[pl.ds(pl.multiple_of(index * rows, rows), rows)]

    def x_copy(index, slot, dev):
        return remote(xrow(index), xrow(index), x_send.at[slot], x_recv.at[index], (s, dev))

    def w_copy(src, index, slot, dev):
        return remote(src, wrow(index), w_send.at[slot], w_recv.at[index], (s, dev))

    barrier = pltpu.get_barrier_semaphore()
    for d in range(1, S * T):
        other = (s * T + t + d) % (S * T)
        pl.semaphore_signal(barrier, inc=1, device_id=(other // T, other % T), device_id_type=MESH)
    loads = [
        pltpu.make_async_copy(wk_hbm, wk, load.at[0]),
        pltpu.make_async_copy(wv_hbm, wv, load.at[1]),
        pltpu.make_async_copy(wq_hbm, wq, load.at[2]),
        pltpu.make_async_copy(wo_hbm, wrow(t), load.at[3]),
    ]
    for copy in loads:
        copy.start()

    xg[pl.ds(pl.multiple_of(t * R, R), R)] = scaled_rows(act[...].astype(f32), gain_in[...])
    pl.semaphore_wait(barrier, S * T - 1)
    for e in range(1, Y):
        go(x_copy(t, e, ((y + e) % Y) * 2 + c))
    go(x_copy(t, 0, partner))
    high = lax.broadcasted_iota(jnp.int32, (B, half), 0)
    low = lax.broadcasted_iota(jnp.int32, (B, half), 1)
    tri[...] = (high > low).astype(f32).astype(bf16)
    for e in range(1, Y):
        came = ((y + e) % Y) * 2 + c
        x_copy(came, 0, partner).wait_recv()
        go(x_copy(came, Y + e - 1, partner))
    for copy in loads:
        copy.wait()
    for e in range(1, Y):
        go(w_copy(wrow(t), t, e, ((y + e) % Y) * 2 + c))
    x_copy(partner, 0, partner).wait_recv()
    for e in range(1, Y):
        x_copy(((y + e) % Y) * 2 + 1 - c, 0, partner).wait_recv()

    rows_all = xg[...]
    keys = jnp.dot(rows_all, wk[...], preferred_element_type=f32).astype(bf16)
    values = jnp.dot(rows_all, wv[...], preferred_element_type=f32).astype(bf16)
    for i in range(H):
        cols = slice(i * dh, (i + 1) * dh)
        kvs[i] = jnp.concatenate([keys[:, cols], values[:, cols]], axis=1)
    for d in range(1, H):
        hd = (h + d) % H
        go(remote(kvs.at[hd], kv.at[s], kv_send.at[d], kv_recv.at[s], (hd * G + g, t)))
    for e in range(1, G):
        remote(
            kvs.at[h], kv.at[s], kv_relay.at[h * (G - 1) + e - 1], kv_recv.at[s], (h * G + (g + e) % G, t)
        ).start()
    kv[s] = kvs[h]
    queries = jnp.dot(rows_all, wq[...], preferred_element_type=f32).astype(bf16)
    for i in range(H):
        cols = slice(i * dh, (i + 1) * dh)
        qs[i] = jnp.concatenate([queries[:half, cols], queries[half:, cols]], axis=1)
    for d in range(1, H):
        hd = (h + d) % H
        go(remote(qs.at[hd], qr.at[s // G], q_send.at[d], q_recv.at[s // G], (hd * G + gq, t)))

    own_q = remote(qs.at[h], qr.at[s // G], q_send.at[0], q_recv.at[s // G], (h * G + gq, t))

    @pl.when(gq != g)
    def _():
        own_q.start()

    @pl.when(gq == g)
    def _():
        qr[s // G] = qs[h]

    def kv_wait(j):
        remote(kvs.at[0], kv.at[j], kv_send.at[0], kv_recv.at[j], (s, t)).wait_recv()

    def relays(k):
        j = k * G + g
        return [
            remote(
                kv.at[j], kv.at[j], kv_relay.at[k * (G - 1) + e - 1], kv_recv.at[j], (h * G + (g + e) % G, t)
            )
            for e in range(1, G)
        ]

    def relay(k):
        @pl.when(k != h)
        def _():
            kv_wait(k * G + g)
            for copy in relays(k):
                copy.start()

    offset = off[h] * log2e
    factor = dh ** (-0.5) * log2e

    def piece(i, block, width, causal):
        key_tile = kv[block, :width]
        z = lax.dot_general(qpad[i], key_tile, (((1,), (1,)), ((), ())), preferred_element_type=f32)
        z = z * factor + offset
        keep = jnp.maximum(jnp.log2(1.0 + jnp.exp2(jnp.minimum(z, 100.0))), z)
        if causal:
            query_pos = i * half + lax.broadcasted_iota(jnp.int32, (half, width), 0)
            earlier = lax.broadcasted_iota(jnp.int32, (half, width), 1) < query_pos
            lost = jnp.where(earlier, keep, 0.0)
        else:
            lost = keep
        lost_b = lost.astype(bf16)
        first = jnp.dot(lost_b, tri[:width], preferred_element_type=f32)
        after = first
        if width > half:
            last = jnp.dot(lost_b[:, half:], tri[:half], preferred_element_type=f32)
            after = jnp.concatenate([first, last], axis=1)
        weight = jnp.exp2(z - keep - after)
        if causal:
            weight = jnp.where(earlier, weight, 0.0)
        part = jnp.dot(weight.astype(bf16), key_tile, preferred_element_type=f32)
        total = first[:, :1] + lost[:, :1]
        if causal:
            acc[i] = part
            carry[i] = jnp.broadcast_to(total, carry.shape[1:])
        else:
            before = carry[i]
            acc[i] += jnp.exp2(-before) * part
            carry[i] = before + total

    relay(0)
    for k in range(H):
        b = block_of(k)
        if k + 1 < H:
            relay(k + 1)
        for e in range(1, G):
            kv_wait(k * G + (g + e) % G)

        @pl.when(b != s)
        def _():
            remote(qs.at[0], qr.at[k], q_send.at[0], q_recv.at[k], (s, t)).wait_recv()

        packed = qr[k]
        blank = jnp.zeros((half, dh), bf16)
        qpad[0] = jnp.concatenate([packed[:, :dh], blank], axis=1)
        qpad[1] = jnp.concatenate([packed[:, dh:], blank], axis=1)
        piece(0, b, half, True)
        piece(1, b, B, True)

        def more(step, unused):
            piece(0, b - 1 - step, B, False)
            piece(1, b - 1 - step, B, False)
            return unused

        lax.fori_loop(0, b, more, 0)
        if k == H // 2 - 1:
            go(w_copy(wrow(t), t, 0, partner))
            for e in range(1, Y):
                came = ((y + e) % Y) * 2 + c
                w_copy(wrow(t), came, 0, partner).wait_recv()
                go(w_copy(wrow(came), came, Y + e - 1, partner))
        for r in range(T):
            chunk = acc[r * R // half, pl.ds(r * R % half, R)]
            obuf[k, r] = jnp.concatenate([chunk[: R // 2, dh:], chunk[R // 2 :, dh:]], axis=1).astype(bf16)
        for e in range(1, T):
            r = (t + e) % T
            go(remote(obuf.at[k, r], orecv.at[t * H + h], o_send.at[k * T + e], o_recv.at[t * H + h], (b, r)))
        own_o = remote(obuf.at[k, t], orecv.at[t * H + h], o_send.at[k * T], o_recv.at[t * H + h], (b, t))

        @pl.when(b != s)
        def _():
            own_o.start()

        @pl.when(b == s)
        def _():
            orecv[t * H + h] = obuf[k, t]

    w_copy(wrow(t), partner, 0, partner).wait_recv()
    for e in range(1, Y):
        w_copy(wrow(t), ((y + e) % Y) * 2 + 1 - c, 0, partner).wait_recv()

    for tt in range(T):
        for hh in range(H):

            @pl.when(jnp.logical_or(tt != t, hh * G + gq != s))
            def _():
                e = tt * H + hh
                remote(obuf.at[0, 0], orecv.at[e], o_send.at[0], o_recv.at[e], (s, t)).wait_recv()

    for p in range(T * H // 2):
        one, two = orecv[2 * p], orecv[2 * p + 1]
        cols = slice(2 * p * dh, (2 * p + 2) * dh)
        att[: R // 2, cols] = jnp.concatenate([one[:, :dh], two[:, :dh]], axis=1)
        att[R // 2 :, cols] = jnp.concatenate([one[:, dh:], two[:, dh:]], axis=1)
    projected = jnp.dot(att[...], wg[...], preferred_element_type=f32)
    out[...] = scaled_rows(projected, gain_out[...])

    for copy in started:
        copy.wait_send()
    for k in range(H):
        for copy in relays(k):
            copy.wait_send()

    @pl.when(gq != g)
    def _():
        own_q.wait_send()

    for k in range(H):
        b = block_of(k)

        @pl.when(b != s)
        def _():
            remote(obuf.at[k, t], orecv.at[t * H + h], o_send.at[k * T], o_recv.at[t * H + h], (b, t)).wait_send()


def solution(mesh):
    S, T = mesh.shape["sp"], mesh.shape["tp"]

    def local(act, gain_in, wq, wk, wv, off, wo, gain_out):
        R, D = act.shape
        H = off.shape[0]
        dh = wq.shape[1] // H
        G = S // H
        B = R * T
        half = B // 2
        vmem = pl.BlockSpec(memory_space=pltpu.VMEM)
        hbm = pl.BlockSpec(memory_space=pl.ANY)
        smem = pl.BlockSpec(memory_space=pltpu.SMEM)
        dma = pltpu.SemaphoreType.DMA
        lanes = 2 * dh
        return pl.pallas_call(
            functools.partial(layer_kernel, S, T, H, dh),
            out_shape=jax.ShapeDtypeStruct((R, D), bf16),
            in_specs=[vmem, vmem, hbm, hbm, hbm, smem, hbm, vmem],
            out_specs=vmem,
            scratch_shapes=[
                pltpu.VMEM(wq.shape, bf16),
                pltpu.VMEM(wk.shape, bf16),
                pltpu.VMEM(wv.shape, bf16),
                pltpu.VMEM((B, D), bf16),
                pltpu.VMEM((wo.shape[0] * T, D), bf16),
                pltpu.VMEM((H, B, lanes), bf16),
                pltpu.VMEM((H, half, lanes), bf16),
                pltpu.VMEM((S, B, lanes), bf16),
                pltpu.VMEM((H, half, lanes), bf16),
                pltpu.VMEM((2, half, lanes), bf16),
                pltpu.VMEM((B, half), bf16),
                pltpu.VMEM((2, half, lanes), f32),
                pltpu.VMEM((2, half, lanes), f32),
                pltpu.VMEM((H, T, R // 2, lanes), bf16),
                pltpu.VMEM((T * H, R // 2, lanes), bf16),
                pltpu.VMEM((R, T * H * dh), bf16),
                dma((T,)),
                dma((T,)),
                dma((T,)),
                dma((T,)),
                dma((H,)),
                dma((H * (G - 1),)),
                dma((S,)),
                dma((H,)),
                dma((H,)),
                dma((H * T,)),
                dma((T * H,)),
                dma((4,)),
            ],
            compiler_params=pltpu.CompilerParams(collective_id=0, has_side_effects=True, vmem_limit_bytes=50 * 2**20),
        )(act, gain_in.reshape(1, D), wq, wk, wv, off, wo, gain_out.reshape(1, D))

    in_specs = (
        P(("sp", "tp"), None),
        P(),
        P(None, "tp"),
        P(None, "tp"),
        P(None, "tp"),
        P("tp"),
        P("tp", None),
        P(),
    )
    out_specs = P(("sp", "tp"), None)
    return jax.shard_map(local, mesh=mesh, in_specs=in_specs, out_specs=out_specs, check_vma=False)
```

profile of v0, /device:TPU:129, one launch (start us, length us, event | category | flops | bytes accessed | tf_op | source)
XLA Modules:
  0.0 186.3 jit_solution(10666125616565824456)
XLA Ops:
  0.0 0.0 copy-start.7
  0.0 0.7 copy-done.7
  0.7 0.0 copy-start
  0.7 0.9 copy-done
  1.6 0.0 copy-start.1
  1.6 0.9 copy-done.1
  2.6 0.0 copy-start.2
  2.6 0.9 copy-done.2
  3.5 0.0 copy-start.3
  3.5 0.9 copy-done.3
  4.5 0.0 copy-start.4
  4.5 0.9 copy-done.4
  5.4 0.0 copy-start.5
  5.4 0.7 copy-done.5
  6.1 0.0 copy-start.6
  6.1 0.7 copy-done.6
  6.7 178.9 %shard_map.82 = bf16[64,1024]{1,0:T(8,128)(2,1)S(1)} custom-call(bf16[64,1024]{1,0:T(8,128)(2,1)S(1)} %copy-done.4, f32[1,1024]{1,0:T(1,128)S(1)} %bitcast.2, bf16[1024,128]{1,0:T(8,128)(2,1)S(1)} %copy-done, bf16[1024,128]{1,0:T(8,128)(2,1)S(1)} %copy-done.1, bf16[1024,128]{1,0:T(8,128)(2,1)S(1)} %copy-done.2, f32[2]{0:T(128)S(1)} %copy-done.7, ...), custom_call_target="tpu_custom_call" | custom-call | tf_op jit(solution)/shard_map/pallas_call | solution.py:327
  185.7 0.7 copy.10
Async XLA Ops:
  0.0 0.7 copy-start.7
  0.7 0.9 copy-start
  1.6 0.9 copy-start.1
  2.6 0.9 copy-start.2
  3.5 0.9 copy-start.3
  4.5 0.9 copy-start.4
  5.4 0.7 copy-start.5
  6.1 0.7 copy-start.6
where the time goes:
time: 187 us; the launch traced here: 186 us
  Pallas kernels  179 us (96%)
  local copies, waits for them, and re-layouts  7.39 us (4%)
    pallas_call x1, Pallas kernels, local(): pl.pallas_call(functools.partial(layer_kernel, S, T, H, dh), out_shape=ja...  179 us
    unnamed x17, local copies, waits for them, and re-layouts  7.39 us

commit v1 on v0

v1 whole, which is shorter than its diff:
```python
import functools

import jax
import jax.numpy as jnp
from jax import lax
from jax.experimental import pallas as pl
from jax.experimental.pallas import tpu as pltpu
from jax.sharding import PartitionSpec as P

epsilon = 1e-06
log2e = 1.4426950408889634
MESH = pl.DeviceIdType.MESH
f32 = jnp.float32
bf16 = jnp.bfloat16
XS = 4
ZMAX = 63.0


def scaled_rows(widened, row_gain):
    spread = jnp.mean(widened * widened, axis=-1, keepdims=True)
    return (widened * lax.rsqrt(spread + epsilon) * row_gain).astype(bf16)


def layer_kernel(
    S,
    T,
    H,
    dh,
    act,
    gain_in,
    wq_hbm,
    wk_hbm,
    wv_hbm,
    off,
    wo_hbm,
    gain_out,
    out,
    wq,
    wk,
    wv,
    xg,
    wg,
    perm,
    kvb,
    qb,
    kvr,
    qr,
    offt,
    ws,
    acc,
    obuf,
    orecv,
    heads,
    x_send,
    x_recv,
    w_send,
    w_recv,
    kv_send,
    kv_recv,
    q_send,
    q_recv,
    o_send,
    o_recv,
    load,
):
    R = act.shape[0]
    B = R * T
    W = B // 2
    rows = wo_hbm.shape[0]
    Z = S // XS
    half_z = Z // 2
    s = lax.axis_index("sp")
    t = lax.axis_index("tp")
    z, x = s // XS, s % XS
    h = z // half_z
    mz = Z - 1 - z
    kz = jnp.where(h == 0, z, mz)
    y, c = t // 2, t % 2
    partner = y * 2 + 1 - c
    Y = T // 2

    def remote(src, dst, send, recv, dev):
        return pltpu.make_async_remote_copy(
            src_ref=src, dst_ref=dst, send_sem=send, recv_sem=recv, device_id=dev, device_id_type=MESH
        )

    started = []

    def go(copy):
        copy.start()
        started.append(copy)
        return copy

    def xrow(index):
        return xg.at[pl.ds(pl.multiple_of(index * R, R), R)]

    def wrow(index):
        return wg.at[pl.ds(pl.multiple_of(index * rows, rows), rows)]

    def x_copy(index, slot, dev):
        return remote(xrow(index), xrow(index), x_send.at[slot], x_recv.at[index], (s, dev))

    def w_copy(src, index, slot, dev):
        return remote(src, wrow(index), w_send.at[slot], w_recv.at[index], (s, dev))

    barrier = pltpu.get_barrier_semaphore()
    for d in range(1, S * T):
        other = (s * T + t + d) % (S * T)
        pl.semaphore_signal(barrier, inc=1, device_id=(other // T, other % T), device_id_type=MESH)
    loads = [
        pltpu.make_async_copy(wk_hbm, wk, load.at[0]),
        pltpu.make_async_copy(wv_hbm, wv, load.at[1]),
        pltpu.make_async_copy(wq_hbm, wq, load.at[2]),
        pltpu.make_async_copy(wo_hbm, wrow(t), load.at[3]),
    ]
    for copy in loads:
        copy.start()

    xg[pl.ds(pl.multiple_of(t * R, R), R)] = scaled_rows(act[...].astype(f32), gain_in[...])
    pl.semaphore_wait(barrier, S * T - 1)
    for e in range(1, Y):
        go(x_copy(t, e, ((y + e) % Y) * 2 + c))
    go(x_copy(t, 0, partner))

    token = lax.broadcasted_iota(jnp.int32, (B, B), 0)
    place = lax.broadcasted_iota(jnp.int32, (B, B), 1)
    perm[...] = (token == (place & (T - 1)) * R + (place >> (T.bit_length() - 1))).astype(f32).astype(bf16)
    whole = jnp.broadcast_to(off[h] * log2e, (16, B)).astype(f32)
    high = whole.astype(bf16).astype(f32)
    middle = (whole - high).astype(bf16).astype(f32)
    low = whole - high - middle
    part_row = lax.broadcasted_iota(jnp.int32, (16, B), 0)
    offt[...] = jnp.where(
        part_row == 0, high, jnp.where(part_row == 1, middle, jnp.where(part_row == 2, low, 0.0))
    ).astype(bf16)

    for e in range(1, Y):
        came = ((y + e) % Y) * 2 + c
        x_copy(came, 0, partner).wait_recv()
        go(x_copy(came, Y + e - 1, partner))
    for copy in loads:
        copy.wait()
    for e in range(1, Y):
        go(w_copy(wrow(t), t, e, ((y + e) % Y) * 2 + c))
    x_copy(partner, 0, partner).wait_recv()
    for e in range(1, Y):
        x_copy(((y + e) % Y) * 2 + 1 - c, 0, partner).wait_recv()

    rows_all = xg[...]
    keys = jnp.dot(rows_all, wk[...], preferred_element_type=f32).astype(bf16).astype(f32)
    values = jnp.dot(rows_all, wv[...], preferred_element_type=f32).astype(bf16).astype(f32)
    turned = jnp.concatenate([keys.T, values.T], axis=0).astype(bf16)
    placed = jnp.dot(turned, perm[...], preferred_element_type=f32)
    keys_placed = placed[: H * dh].T
    for i in range(H):
        cols = slice(i * dh, (i + 1) * dh)
        kvb[i, :W] = jnp.concatenate([keys_placed[:W, cols], keys_placed[W:, cols]], axis=1).astype(bf16)
        for part in range(4):
            piece = placed[(H + i) * dh : (H + i + 1) * dh, part * 128 : (part + 1) * 128]
            kvb[i, W + part * dh : W + (part + 1) * dh] = piece.astype(bf16)

    def kv_copy(src, row, col, slot, dev):
        return remote(src, kvr.at[row, col], kv_send.at[slot], kv_recv.at[row * XS + col], (dev, t))

    go(kv_copy(kvb.at[1 - h], h, x, 0, mz * XS + x))
    for e in (1, 3, 2):
        go(kv_copy(kvb.at[h], h, x, e, z * XS + (x + e) % XS))
    kvr[h, x] = kvb[h]

    queries = jnp.dot(rows_all, wq[...], preferred_element_type=f32) * (dh ** (-0.5) * log2e)
    q_turned = queries.T.astype(bf16)
    for i in range(H):
        qb[i] = q_turned[i * dh : (i + 1) * dh]
    qr[z] = qb[h]

    def q_copy(i, depth):
        dev = depth if i == 0 else Z - 1 - depth
        return dev, remote(qb.at[i], qr.at[z], q_send.at[i * half_z + depth], q_recv.at[z], (dev * XS + x, t))

    def q_extra(i):
        dev = mz if i == 0 else z
        return remote(qb.at[i], qr.at[Z], q_send.at[H * half_z + i], q_recv.at[Z], (dev * XS + XS - 1 - x, t))

    def each_q(act_on):
        @pl.when(h == 1)
        def _():
            for i in range(H):
                act_on(q_extra(i))

        for depth in range(half_z - 1, -1, -1):
            for i in range(H):
                dev, copy = q_copy(i, depth)

                @pl.when(jnp.logical_and(depth <= z, dev != z))
                def _():
                    act_on(copy)

    each_q(lambda copy: copy.start())

    def kv_wait(row, col):
        @pl.when(jnp.logical_or(row != h, col != x))
        def _():
            remote(kvb.at[0], kvr.at[row, col], kv_send.at[0], kv_recv.at[row * XS + col], (s, t)).wait_recv()

    def q_wait(slot):
        @pl.when(slot != z)
        def _():
            remote(qb.at[0], qr.at[slot], q_send.at[0], q_recv.at[slot], (s, t)).wait_recv()

    lane = lax.broadcasted_iota(jnp.int32, (16, 128), 1)
    ones = (lane < 3).astype(f32).astype(bf16)
    zeros = jnp.zeros((dh, W), bf16)
    pad = jnp.zeros((112, W), bf16)

    def weigh(row, col, slot, j, masked):
        sl = slice(j * W, (j + 1) * W)
        run = jnp.ones((8, W), f32)
        if masked:
            ahead = (
                lax.broadcasted_iota(jnp.int32, (8, W), 1)
                + j * W
                - R * lax.broadcasted_iota(jnp.int32, (8, W), 0)
            )
        lhs = jnp.concatenate([kvr[row, col, :W], jnp.tile(ones, (W // 16, 1))], axis=1)
        for part in (1, 0):
            q = qr[slot, :, sl]
            stack = [q, zeros] if part == 0 else [zeros, q]
            rhs = jnp.concatenate(stack + [offt[:, sl], pad], axis=0)
            score = jnp.minimum(jnp.dot(lhs, rhs, preferred_element_type=f32), ZMAX)
            for v in range(W // 8 - 2, -1, -2):
                e0 = jnp.exp2(score[8 * v : 8 * v + 8])
                e1 = jnp.exp2(score[8 * v + 8 : 8 * v + 16])
                if masked:
                    place_v = part * (W // 8) + v
                    e0 = jnp.where(ahead > place_v, e0, 0.0)
                    e1 = jnp.where(ahead > place_v + 1, e1, 0.0)
                u0, u1 = 1.0 + e0, 1.0 + e1
                left = run * (1.0 / (u0 * u1))
                first = e0 * left
                second = e1 * (u0 * left)
                run = left
                base = part * W + 8 * v
                ws[j, base : base + 16] = jnp.concatenate([first, second], axis=0).astype(bf16)
        later = [None] * 8
        total = jnp.ones((1, W), f32)
        for i in range(7, -1, -1):
            later[i] = total
            total = total * run[i : i + 1]
        return jnp.concatenate(later + later, axis=0).astype(bf16), total

    def gather(row, col, j, later, total, first):
        sl = slice(j * W, (j + 1) * W)
        weight = (ws[j].reshape(B // 16, 16, W) * later[None]).reshape(B, W)
        vt = jnp.concatenate([kvr[row, col, W + p * dh : W + (p + 1) * dh] for p in range(4)], axis=1)
        part = jnp.dot(vt, weight, preferred_element_type=f32)
        acc[:, sl] = part if first else acc[:, sl] * total + part

    def unit_of(turn):
        j = jnp.where(h == 0, turn, Z - 2 - turn)
        is_low = j < Z - 1 - kz
        zq = jnp.where(is_low, kz + 1 + j, j + 1)
        return jnp.where(is_low, 0, 1), zq

    def send_out(u, row, block, kept):
        lanes = lax.broadcasted_iota(jnp.int32, (dh // 2, 128), 1) < dh
        lanes_t = lax.broadcasted_iota(jnp.int32, (16, 128), 1) < dh
        top = lax.broadcasted_iota(jnp.int32, (16, 128), 0) == 0
        for g in range(T // 2):
            cols = slice(g * 128, (g + 1) * 128)
            a, b = acc[: dh // 2, cols], acc[dh // 2 :, cols]
            ar, br = pltpu.roll(a, dh, 1), pltpu.roll(b, dh, 1)
            j, inner = g * 128 // W, g * 128 % W
            tt = jnp.broadcast_to(kept[j][:, inner : inner + 128], (16, 128))
            tr = pltpu.roll(tt, dh, 1)
            for odd in range(2):
                body = jnp.where(lanes, ar, b) if odd else jnp.where(lanes, a, br)
                fac = jnp.where(lanes_t, tr, tt) if odd else jnp.where(lanes_t, tt, tr)
                fac_high = fac.astype(bf16).astype(f32)
                tail = jnp.where(top, fac_high, fac - fac_high)
                obuf[u, 2 * g + odd] = jnp.concatenate([body, tail], axis=0).astype(bf16)
        dst = row * T * H + t * H + h
        for e in range(1, T):
            r = (t + e) % T
            remote(obuf.at[u, r], orecv.at[dst], o_send.at[u * T + e], o_recv.at[dst], (block, r)).start()

        @pl.when(block != s)
        def _():
            remote(obuf.at[u, t], orecv.at[dst], o_send.at[u * T], o_recv.at[dst], (block, t)).start()

        @pl.when(block == s)
        def _():
            orecv[dst] = obuf[u, t]

    def key_row(row):
        return jnp.where(row == 0, kz, Z - 1 - kz)

    def self_unit(u, row, fresh):
        n = jnp.where(row == 0, x, XS - 1 - x)
        slot = jnp.where(row == 0, kz, Z)
        q_wait(slot)
        for j in range(2):
            acc[:, j * W : (j + 1) * W] = jnp.zeros((dh, W), f32)

        def step(col, kept):
            if fresh:
                kv_wait(row, col)
            nxt = []
            found = []
            for j in range(2):
                found.append(weigh(row, col, slot, j, False))
            for j in range(2):
                gather(row, col, j, *found[j], False)
                nxt.append(kept[j] * found[j][1])
            return tuple(nxt)

        one = jnp.ones((1, W), f32)
        kept = lax.fori_loop(0, n, step, (one, one))
        if fresh:
            kv_wait(row, n)
        found = [weigh(row, n, slot, j, True) for j in range(2)]
        for j in range(2):
            gather(row, n, j, *found[j], False)
        send_out(u, key_row(row), key_row(row) * XS + n, [kept[j] * found[j][1] for j in range(2)])
        return n

    n = self_unit(0, h, True)
    for col in range(XS):

        @pl.when(col > n)
        def _():
            kv_wait(h, col)

    kv_wait(1 - h, x)
    for e in (1, 3, 2):
        go(kv_copy(kvr.at[1 - h, x], 1 - h, x, 3 + e, z * XS + (x + e) % XS))

    turn_over = jnp.where(h == 0, Z - 1 - kz, kz)

    def mirrored():
        for e in range(1, XS):
            kv_wait(1 - h, (x + e) % XS)

    def full(turn, unused):
        row, zq = unit_of(turn)

        @pl.when(turn == turn_over)
        def _():
            mirrored()

        later_use = jnp.logical_and(row != h, zq > Z - 1 - kz)

        @pl.when(jnp.logical_not(later_use))
        def _():
            q_wait(zq)

        kept = [None, None]
        waiting = None
        for col in range(XS):
            for j in range(2):
                later, total = weigh(row, col, zq, j, False)
                if waiting is not None:
                    gather(*waiting)
                waiting = (row, col, j, later, total, col == 0)
                kept[j] = total if col == 0 else kept[j] * total
        gather(*waiting)
        send_out(turn + 1, key_row(row), zq * XS + x, kept)
        return unused

    lax.fori_loop(0, 3, full, 0)
    go(w_copy(wrow(t), t, 0, partner))
    for e in range(1, Y):
        came = ((y + e) % Y) * 2 + c
        w_copy(wrow(t), came, 0, partner).wait_recv()
        go(w_copy(wrow(came), came, Y + e - 1, partner))
    lax.fori_loop(3, Z - 1, full, 0)

    @pl.when(turn_over == Z - 1)
    def _():
        mirrored()

    self_unit(Z, 1 - h, False)

    w_copy(wrow(t), partner, 0, partner).wait_recv()
    for e in range(1, Y):
        w_copy(wrow(t), ((y + e) % Y) * 2 + 1 - c, 0, partner).wait_recv()

    for hh in range(T * H):
        heads[hh] = jnp.zeros((dh // 2, 128), f32)

    def combine(r, unused):
        for hh in range(T * H):

            @pl.when(jnp.logical_or(r != kz, hh != t * H + h))
            def _():
                e = r * T * H + hh
                remote(obuf.at[0, 0], orecv.at[e], o_send.at[0], o_recv.at[e], (s, t)).wait_recv()

        for hh in range(T * H):
            got = orecv[r * T * H + hh].astype(f32)
            fac = got[dh // 2 : dh // 2 + 1] + got[dh // 2 + 1 : dh // 2 + 2]
            heads[hh] = heads[hh] * fac + got[: dh // 2]
        return unused

    lax.fori_loop(0, z + 1, combine, 0)

    lhs, rhs = [], []
    for q in range(T * H // 4):
        both = jnp.concatenate([heads[4 * q + a] for a in range(4)], axis=0).T
        for e in range(2):
            lhs.append(both[e * dh : (e + 1) * dh].astype(bf16))
            for a in range(4):
                base = (4 * q + a) * dh + e * (dh // 2)
                rhs.append(wg[base : base + dh // 2])
    projected = jnp.dot(
        jnp.concatenate(lhs, axis=1), jnp.concatenate(rhs, axis=0), preferred_element_type=f32
    )
    out[...] = scaled_rows(projected, gain_out[...])

    for copy in started:
        copy.wait_send()
    each_q(lambda copy: copy.wait_send())

    def sent(u, block):
        for e in range(1, T):
            remote(obuf.at[u, 0], orecv.at[0], o_send.at[u * T + e], o_recv.at[0], (s, t)).wait_send()

        @pl.when(block != s)
        def _():
            remote(obuf.at[u, 0], orecv.at[0], o_send.at[u * T], o_recv.at[0], (s, t)).wait_send()

    def self_block(row):
        return key_row(row) * XS + jnp.where(row == 0, x, XS - 1 - x)

    sent(0, self_block(h))
    sent(Z, self_block(1 - h))

    def sent_full(turn, unused):
        sent(turn + 1, unit_of(turn)[1] * XS + x)
        return unused

    lax.fori_loop(0, Z - 1, sent_full, 0)


def solution(mesh):
    S, T = mesh.shape["sp"], mesh.shape["tp"]

    def local(act, gain_in, wq, wk, wv, off, wo, gain_out):
        R, D = act.shape
        H = off.shape[0]
        dh = wq.shape[1] // H
        B = R * T
        Z = S // XS
        vmem = pl.BlockSpec(memory_space=pltpu.VMEM)
        hbm = pl.BlockSpec(memory_space=pl.ANY)
        smem = pl.BlockSpec(memory_space=pltpu.SMEM)
        dma = pltpu.SemaphoreType.DMA
        return pl.pallas_call(
            functools.partial(layer_kernel, S, T, H, dh),
            out_shape=jax.ShapeDtypeStruct((R, D), bf16),
            in_specs=[vmem, vmem, hbm, hbm, hbm, smem, hbm, vmem],
            out_specs=vmem,
            scratch_shapes=[
                pltpu.VMEM(wq.shape, bf16),
                pltpu.VMEM(wk.shape, bf16),
                pltpu.VMEM(wv.shape, bf16),
                pltpu.VMEM((B, D), bf16),
                pltpu.VMEM((wo.shape[0] * T, D), bf16),
                pltpu.VMEM((B, B), bf16),
                pltpu.VMEM((H, B, 128), bf16),
                pltpu.VMEM((H, dh, B), bf16),
                pltpu.VMEM((2, XS, B, 128), bf16),
                pltpu.VMEM((Z + 1, dh, B), bf16),
                pltpu.VMEM((16, B), bf16),
                pltpu.VMEM((2, B, B // 2), bf16),
                pltpu.VMEM((dh, B), f32),
                pltpu.VMEM((Z + 1, T, dh // 2 + 16, 128), bf16),
                pltpu.VMEM((Z * T * H, dh // 2 + 16, 128), bf16),
                pltpu.VMEM((T * H, dh // 2, 128), f32),
                dma((T,)),
                dma((T,)),
                dma((T,)),
                dma((T,)),
                dma((8,)),
                dma((2 * XS,)),
                dma((H * Z // 2 + H,)),
                dma((Z + 1,)),
                dma(((Z + 1) * T,)),
                dma((Z * T * H,)),
                dma((4,)),
            ],
            compiler_params=pltpu.CompilerParams(collective_id=0, has_side_effects=True, vmem_limit_bytes=50 * 2**20),
        )(act, gain_in.reshape(1, D), wq, wk, wv, off, wo, gain_out.reshape(1, D))

    in_specs = (
        P(("sp", "tp"), None),
        P(),
        P(None, "tp"),
        P(None, "tp"),
        P(None, "tp"),
        P("tp"),
        P("tp", None),
        P(),
    )
    out_specs = P(("sp", "tp"), None)
    return jax.shard_map(local, mesh=mesh, in_specs=in_specs, out_specs=out_specs, check_vma=False)
```

time: 187 us -> 91.3 us (0.49)
  the two profiles are of different devices: /device:TPU:129 before, /device:TPU:229 now
where the time goes in v1:
time: 91.3 us; the launch traced here: 91.1 us
  Pallas kernels  83.7 us (92%)
  local copies, waits for them, and re-layouts  7.39 us (8%)
    pallas_call x1, Pallas kernels, local(): pl.pallas_call(functools.partial(layer_kernel, S, T, H, dh), out_shape=ja...  83.7 us
    unnamed x17, local copies, waits for them, and re-layouts  7.39 us

profile of v1, /device:TPU:229, one launch (start us, length us, event | category | flops | bytes accessed | tf_op | source)
XLA Modules:
  0.0 91.1 jit_solution(1063668449481859230)
XLA Ops:
  0.0 0.0 copy-start.7
  0.0 0.7 copy-done.7
  0.7 0.0 copy-start
  0.7 0.9 %copy-done = bf16[1024,128]{1,0:T(8,128)(2,1)S(1)} copy-done((bf16[1024,128]{1,0:T(8,128)(2,1)S(1)}, bf16[1024,128]{1,0:T(8,128)(2,1)}, u32[]{:S(2)}) %copy-start) | copy-done | bytes 262168
  1.6 0.0 copy-start.1
  1.6 0.9 %copy-done.1 = bf16[1024,128]{1,0:T(8,128)(2,1)S(1)} copy-done((bf16[1024,128]{1,0:T(8,128)(2,1)S(1)}, bf16[1024,128]{1,0:T(8,128)(2,1)}, u32[]{:S(2)}) %copy-start.1) | copy-done | bytes 262168
  2.6 0.0 copy-start.2
  2.6 0.9 %copy-done.2 = bf16[1024,128]{1,0:T(8,128)(2,1)S(1)} copy-done((bf16[1024,128]{1,0:T(8,128)(2,1)S(1)}, bf16[1024,128]{1,0:T(8,128)(2,1)}, u32[]{:S(2)}) %copy-start.2) | copy-done | bytes 262168
  3.5 0.0 copy-start.3
  3.5 0.9 %copy-done.3 = bf16[128,1024]{1,0:T(8,128)(2,1)S(1)} copy-done((bf16[128,1024]{1,0:T(8,128)(2,1)S(1)}, bf16[128,1024]{1,0:T(8,128)(2,1)}, u32[]{:S(2)}) %copy-start.3) | copy-done | bytes 262168
  4.5 0.0 copy-start.4
  4.5 0.9 copy-done.4
  5.4 0.0 copy-start.5
  5.4 0.7 copy-done.5
  6.1 0.0 copy-start.6
  6.1 0.7 copy-done.6
  6.7 83.7 %shard_map.82 = bf16[64,1024]{1,0:T(8,128)(2,1)S(1)} custom-call(bf16[64,1024]{1,0:T(8,128)(2,1)S(1)} %copy-done.4, f32[1,1024]{1,0:T(1,128)S(1)} %bitcast.2, bf16[1024,128]{1,0:T(8,128)(2,1)S(1)} %copy-done, bf16[1024,128]{1,0:T(8,128)(2,1)S(1)} %copy-done.1, bf16[1024,128]{1,0:T(8,128)(2,1)S(1)} %copy-done.2, f32[2]{0:T(128)S(1)} %copy-done.7, ...), custom_call_target="tpu_custom_call" | custom-call | tf_op jit(solution)/shard_map/pallas_call | solution.py:457
  90.4 0.7 copy.10
Async XLA Ops:
  0.0 0.7 copy-start.7
  0.7 0.9 %copy-start = (bf16[1024,128]{1,0:T(8,128)(2,1)S(1)}, bf16[1024,128]{1,0:T(8,128)(2,1)}, u32[]{:S(2)}) copy-start(bf16[1024,128]{1,0:T(8,128)(2,1)} %wq_hbm.1) | copy-start | bytes 786436
  1.6 0.9 %copy-start.1 = (bf16[1024,128]{1,0:T(8,128)(2,1)S(1)}, bf16[1024,128]{1,0:T(8,128)(2,1)}, u32[]{:S(2)}) copy-start(bf16[1024,128]{1,0:T(8,128)(2,1)} %wk_hbm.1) | copy-start | bytes 786436
  2.6 0.9 %copy-start.2 = (bf16[1024,128]{1,0:T(8,128)(2,1)S(1)}, bf16[1024,128]{1,0:T(8,128)(2,1)}, u32[]{:S(2)}) copy-start(bf16[1024,128]{1,0:T(8,128)(2,1)} %wv_hbm.1) | copy-start | bytes 786436
  3.5 0.9 %copy-start.3 = (bf16[128,1024]{1,0:T(8,128)(2,1)S(1)}, bf16[128,1024]{1,0:T(8,128)(2,1)}, u32[]{:S(2)}) copy-start(bf16[128,1024]{1,0:T(8,128)(2,1)} %wo_hbm.1) | copy-start | bytes 786436
  4.5 0.9 copy-start.4
  5.4 0.7 copy-start.5
  6.1 0.7 copy-start.6

commit v2 on v1

--- a/solution.py
+++ b/solution.py
@@ -26,15 +26,18 @@
     T,
     H,
     dh,
-    act,
-    gain_in,
+    act_hbm,
+    gain_in_hbm,
     wq_hbm,
     wk_hbm,
     wv_hbm,
     off,
     wo_hbm,
+    gain_out_hbm,
+    out,
+    act,
+    gain_in,
     gain_out,
-    out,
     wq,
     wk,
     wv,
@@ -50,6 +53,8 @@
     acc,
     obuf,
     orecv,
+    tbuf,
+    trecv,
     heads,
     x_send,
     x_recv,
@@ -61,6 +66,8 @@
     q_recv,
     o_send,
     o_recv,
+    t_send,
+    t_recv,
     load,
 ):
     R = act.shape[0]
@@ -103,23 +110,37 @@
     def w_copy(src, index, slot, dev):
         return remote(src, wrow(index), w_send.at[slot], w_recv.at[index], (s, dev))
 
-    barrier = pltpu.get_barrier_semaphore()
-    for d in range(1, S * T):
-        other = (s * T + t + d) % (S * T)
-        pl.semaphore_signal(barrier, inc=1, device_id=(other // T, other % T), device_id_type=MESH)
+    early = [
+        pltpu.make_async_copy(act_hbm, act, load.at[4]),
+        pltpu.make_async_copy(gain_in_hbm, gain_in, load.at[5]),
+    ]
+    for copy in early:
+        copy.start()
     loads = [
         pltpu.make_async_copy(wk_hbm, wk, load.at[0]),
         pltpu.make_async_copy(wv_hbm, wv, load.at[1]),
         pltpu.make_async_copy(wq_hbm, wq, load.at[2]),
         pltpu.make_async_copy(wo_hbm, wrow(t), load.at[3]),
+        pltpu.make_async_copy(gain_out_hbm, gain_out, load.at[6]),
     ]
     for copy in loads:
         copy.start()
-
+    barrier = pltpu.get_barrier_semaphore()
+    partners = [(s, (t + d) % T) for d in range(1, T)]
+    partners += [((z + d) % Z * XS + x, t) for d in range(1, Z)]
+    partners += [(z * XS + (x + d) % XS, t) for d in range(1, XS)]
+    partners += [(mz * XS + XS - 1 - x, t)]
+    for other in partners:
+        pl.semaphore_signal(barrier, inc=1, device_id=other, device_id_type=MESH)
+    for copy in early:
+        copy.wait()
     xg[pl.ds(pl.multiple_of(t * R, R), R)] = scaled_rows(act[...].astype(f32), gain_in[...])
-    pl.semaphore_wait(barrier, S * T - 1)
-    for e in range(1, Y):
-        go(x_copy(t, e, ((y + e) % Y) * 2 + c))
+    pl.semaphore_wait(barrier, len(partners))
+    onward = (y + 1 + (Y - 2) * c) % Y
+    behind = (y + Y - 1 - (Y - 2) * c) % Y
+    across = (y + 2) % Y
+    go(x_copy(t, 1, onward * 2 + c))
+    go(x_copy(t, 2, behind * 2 + c))
     go(x_copy(t, 0, partner))
 
     token = lax.broadcasted_iota(jnp.int32, (B, B), 0)
@@ -134,10 +155,13 @@
         part_row == 0, high, jnp.where(part_row == 1, middle, jnp.where(part_row == 2, low, 0.0))
     ).astype(bf16)
 
-    for e in range(1, Y):
-        came = ((y + e) % Y) * 2 + c
-        x_copy(came, 0, partner).wait_recv()
-        go(x_copy(came, Y + e - 1, partner))
+    x_copy(behind * 2 + c, 0, partner).wait_recv()
+    go(x_copy(behind * 2 + c, 3, onward * 2 + c))
+    go(x_copy(behind * 2 + c, 4, partner))
+    x_copy(onward * 2 + c, 0, partner).wait_recv()
+    go(x_copy(onward * 2 + c, 5, partner))
+    x_copy(across * 2 + c, 0, partner).wait_recv()
+    go(x_copy(across * 2 + c, 6, partner))
     for copy in loads:
         copy.wait()
     for e in range(1, Y):
@@ -261,35 +285,42 @@
         zq = jnp.where(is_low, kz + 1 + j, j + 1)
         return jnp.where(is_low, 0, 1), zq
 
+    def o_copies(u, r, e, dst, dev):
+        return (
+            remote(obuf.at[u, r], orecv.at[dst], o_send.at[u * T + e], o_recv.at[dst], dev),
+            remote(tbuf.at[u, r], trecv.at[dst], t_send.at[u * T + e], t_recv.at[dst], dev),
+        )
+
     def send_out(u, row, block, kept):
         lanes = lax.broadcasted_iota(jnp.int32, (dh // 2, 128), 1) < dh
-        lanes_t = lax.broadcasted_iota(jnp.int32, (16, 128), 1) < dh
-        top = lax.broadcasted_iota(jnp.int32, (16, 128), 0) == 0
+        lanes_t = lax.broadcasted_iota(jnp.int32, (8, 128), 1) < dh
         for g in range(T // 2):
             cols = slice(g * 128, (g + 1) * 128)
             a, b = acc[: dh // 2, cols], acc[dh // 2 :, cols]
             ar, br = pltpu.roll(a, dh, 1), pltpu.roll(b, dh, 1)
             j, inner = g * 128 // W, g * 128 % W
-            tt = jnp.broadcast_to(kept[j][:, inner : inner + 128], (16, 128))
+            tt = jnp.broadcast_to(kept[j][:, inner : inner + 128], (8, 128))
             tr = pltpu.roll(tt, dh, 1)
             for odd in range(2):
                 body = jnp.where(lanes, ar, b) if odd else jnp.where(lanes, a, br)
                 fac = jnp.where(lanes_t, tr, tt) if odd else jnp.where(lanes_t, tt, tr)
-                fac_high = fac.astype(bf16).astype(f32)
-                tail = jnp.where(top, fac_high, fac - fac_high)
-                obuf[u, 2 * g + odd] = jnp.concatenate([body, tail], axis=0).astype(bf16)
+                obuf[u, 2 * g + odd] = body.astype(bf16)
+                tbuf[u, 2 * g + odd] = fac[:1]
         dst = row * T * H + t * H + h
         for e in range(1, T):
             r = (t + e) % T
-            remote(obuf.at[u, r], orecv.at[dst], o_send.at[u * T + e], o_recv.at[dst], (block, r)).start()
+            for copy in o_copies(u, r, e, dst, (block, r)):
+                copy.start()
 
         @pl.when(block != s)
         def _():
-            remote(obuf.at[u, t], orecv.at[dst], o_send.at[u * T], o_recv.at[dst], (block, t)).start()
+            for copy in o_copies(u, t, 0, dst, (block, t)):
+                copy.start()
 
         @pl.when(block == s)
         def _():
             orecv[dst] = obuf[u, t]
+            trecv[dst] = tbuf[u, t]
 
     def key_row(row):
         return jnp.where(row == 0, kz, Z - 1 - kz)
@@ -393,12 +424,11 @@
             @pl.when(jnp.logical_or(r != kz, hh != t * H + h))
             def _():
                 e = r * T * H + hh
-                remote(obuf.at[0, 0], orecv.at[e], o_send.at[0], o_recv.at[e], (s, t)).wait_recv()
+                for copy in o_copies(0, 0, 0, e, (s, t)):
+                    copy.wait_recv()
 
         for hh in range(T * H):
-            got = orecv[r * T * H + hh].astype(f32)
-            fac = got[dh // 2 : dh // 2 + 1] + got[dh // 2 + 1 : dh // 2 + 2]
-            heads[hh] = heads[hh] * fac + got[: dh // 2]
+            heads[hh] = heads[hh] * trecv[r * T * H + hh] + orecv[r * T * H + hh].astype(f32)
         return unused
 
     lax.fori_loop(0, z + 1, combine, 0)
@@ -422,11 +452,13 @@
 
     def sent(u, block):
         for e in range(1, T):
-            remote(obuf.at[u, 0], orecv.at[0], o_send.at[u * T + e], o_recv.at[0], (s, t)).wait_send()
+            for copy in o_copies(u, 0, e, 0, (s, t)):
+                copy.wait_send()
 
         @pl.when(block != s)
         def _():
-            remote(obuf.at[u, 0], orecv.at[0], o_send.at[u * T], o_recv.at[0], (s, t)).wait_send()
+            for copy in o_copies(u, 0, 0, 0, (s, t)):
+                copy.wait_send()
 
     def self_block(row):
         return key_row(row) * XS + jnp.where(row == 0, x, XS - 1 - x)
@@ -457,9 +489,12 @@
         return pl.pallas_call(
             functools.partial(layer_kernel, S, T, H, dh),
             out_shape=jax.ShapeDtypeStruct((R, D), bf16),
-            in_specs=[vmem, vmem, hbm, hbm, hbm, smem, hbm, vmem],
+            in_specs=[hbm, hbm, hbm, hbm, hbm, smem, hbm, hbm],
             out_specs=vmem,
             scratch_shapes=[
+                pltpu.VMEM((R, D), bf16),
+                pltpu.VMEM((1, D), f32),
+                pltpu.VMEM((1, D), f32),
                 pltpu.VMEM(wq.shape, bf16),
                 pltpu.VMEM(wk.shape, bf16),
                 pltpu.VMEM(wv.shape, bf16),
@@ -473,8 +508,10 @@
                 pltpu.VMEM((16, B), bf16),
                 pltpu.VMEM((2, B, B // 2), bf16),
                 pltpu.VMEM((dh, B), f32),
-                pltpu.VMEM((Z + 1, T, dh // 2 + 16, 128), bf16),
-                pltpu.VMEM((Z * T * H, dh // 2 + 16, 128), bf16),
+                pltpu.VMEM((Z + 1, T, dh // 2, 128), bf16),
+                pltpu.VMEM((Z * T * H, dh // 2, 128), bf16),
+                pltpu.VMEM((Z + 1, T, 1, 128), f32),
+                pltpu.VMEM((Z * T * H, 1, 128), f32),
                 pltpu.VMEM((T * H, dh // 2, 128), f32),
                 dma((T,)),
                 dma((T,)),
@@ -486,9 +523,11 @@
                 dma((Z + 1,)),
                 dma(((Z + 1) * T,)),
                 dma((Z * T * H,)),
-                dma((4,)),
+                dma(((Z + 1) * T,)),
+                dma((Z * T * H,)),
+                dma((7,)),
             ],
-            compiler_params=pltpu.CompilerParams(collective_id=0, has_side_effects=True, vmem_limit_bytes=50 * 2**20),
+            compiler_params=pltpu.CompilerParams(collective_id=0, has_side_effects=True, vmem_limit_bytes=67043328),
         )(act, gain_in.reshape(1, D), wq, wk, wv, off, wo, gain_out.reshape(1, D))
 
     in_specs = (

time: 91.3 us -> 78.1 us (0.86)
  the two profiles are of different devices: /device:TPU:229 before, /device:TPU:225 now
where the time goes in v2:
time: 78.1 us; the launch traced here: 77.9 us
  Pallas kernels  76.4 us (98%)
  local copies, waits for them, and re-layouts  1.57 us (2%)
    pallas_call x1, Pallas kernels, local(): pl.pallas_call(functools.partial(layer_kernel, S, T, H, dh), out_shape=ja...  76.4 us
    unnamed x1, local copies, waits for them, and re-layouts  1.57 us

profile of v2, /device:TPU:225, one launch (start us, length us, event | category | flops | bytes accessed | tf_op | source)
XLA Modules:
  0.0 77.9 jit_solution(1790382479679530959)
XLA Ops:
  0.0 76.4 %shard_map.82 = bf16[64,1024]{1,0:T(8,128)(2,1)} custom-call(bf16[64,1024]{1,0:T(8,128)(2,1)} %act_hbm.1, f32[1,1024]{1,0:T(1,128)} %bitcast.2, bf16[1024,128]{1,0:T(8,128)(2,1)} %wq_hbm.1, bf16[1024,128]{1,0:T(8,128)(2,1)} %wk_hbm.1, bf16[1024,128]{1,0:T(8,128)(2,1)} %wv_hbm.1, f32[2]{0:T(128)} %off.1, bf16[128,1024]{1,0:T(8,128)(2,1)} %wo_hbm.1, ...), custom_call_target="tpu_custom_call" | custom-call | tf_op jit(solution)/shard_map/pallas_call | solution.py:489
  76.4 1.6 %copy.10 = bf16[64,1024]{1,0:T(8,128)(2,1)} copy(bf16[64,1024]{1,0:T(8,128)(2,1)} %shard_map.82) | data formatting | bytes 262144

commit v3 on v2

--- a/solution.py
+++ b/solution.py
@@ -14,6 +14,7 @@
 bf16 = jnp.bfloat16
 XS = 4
 ZMAX = 63.0
+LAST = 11
 
 
 def scaled_rows(widened, row_gain):
@@ -51,6 +52,9 @@
     offt,
     ws,
     acc,
+    factors,
+    mbuf,
+    offs,
     obuf,
     orecv,
     tbuf,
@@ -64,6 +68,11 @@
     kv_recv,
     q_send,
     q_recv,
+    f_send,
+    m_send,
+    m_recv,
+    off_send,
+    off_recv,
     o_send,
     o_recv,
     t_send,
@@ -75,15 +84,20 @@
     W = B // 2
     rows = wo_hbm.shape[0]
     Z = S // XS
-    half_z = Z // 2
     s = lax.axis_index("sp")
     t = lax.axis_index("tp")
     z, x = s // XS, s % XS
-    h = z // half_z
-    mz = Z - 1 - z
-    kz = jnp.where(h == 0, z, mz)
     y, c = t // 2, t % 2
     partner = y * 2 + 1 - c
+    place_z = (z + 2) % Z
+    g, hl = place_z // 4, place_z % 4
+    kz = 2 * g + c
+    head = 2 * H * y + hl
+    home = hl // H == c
+
+    def spot(group, local):
+        return (4 * group + local + Z - 2) % Z
+
     Y = T // 2
 
     def remote(src, dst, send, recv, dev):
@@ -127,9 +141,12 @@
         copy.start()
     barrier = pltpu.get_barrier_semaphore()
     partners = [(s, (t + d) % T) for d in range(1, T)]
-    partners += [((z + d) % Z * XS + x, t) for d in range(1, Z)]
-    partners += [(z * XS + (x + d) % XS, t) for d in range(1, XS)]
-    partners += [(mz * XS + XS - 1 - x, t)]
+    for d in range(Z):
+        for core in range(2):
+            if d:
+                partners.append(((z + d) % Z * XS + x, 2 * y + core))
+            partners.append(((z + d) % Z * XS + XS - 1 - x, 2 * y + core))
+    partners += [(z * XS + (x + 2) % XS, t), (z * XS + (XS - 1 - x + 2) % XS, t)]
     for other in partners:
         pl.semaphore_signal(barrier, inc=1, device_id=other, device_id_type=MESH)
     for copy in early:
@@ -146,15 +163,10 @@
     token = lax.broadcasted_iota(jnp.int32, (B, B), 0)
     place = lax.broadcasted_iota(jnp.int32, (B, B), 1)
     perm[...] = (token == (place & (T - 1)) * R + (place >> (T.bit_length() - 1))).astype(f32).astype(bf16)
-    whole = jnp.broadcast_to(off[h] * log2e, (16, B)).astype(f32)
-    high = whole.astype(bf16).astype(f32)
-    middle = (whole - high).astype(bf16).astype(f32)
-    low = whole - high - middle
-    part_row = lax.broadcasted_iota(jnp.int32, (16, B), 0)
-    offt[...] = jnp.where(
-        part_row == 0, high, jnp.where(part_row == 1, middle, jnp.where(part_row == 2, low, 0.0))
-    ).astype(bf16)
-
+    for i in range(H):
+        offs[H * c + i] = jnp.broadcast_to(off[i] * log2e, (1, 128)).astype(f32)
+    mine = offs.at[pl.ds(H * c, H)]
+    go(remote(mine, mine, off_send.at[0], off_recv.at[0], (s, partner)))
     x_copy(behind * 2 + c, 0, partner).wait_recv()
     go(x_copy(behind * 2 + c, 3, onward * 2 + c))
     go(x_copy(behind * 2 + c, 4, partner))
@@ -183,53 +195,116 @@
             piece = placed[(H + i) * dh : (H + i + 1) * dh, part * 128 : (part + 1) * 128]
             kvb[i, W + part * dh : W + (part + 1) * dh] = piece.astype(bf16)
 
+    outer = jnp.minimum(z, Z - 1 - z)
+
     def kv_copy(src, row, col, slot, dev):
-        return remote(src, kvr.at[row, col], kv_send.at[slot], kv_recv.at[row * XS + col], (dev, t))
-
-    go(kv_copy(kvb.at[1 - h], h, x, 0, mz * XS + x))
-    for e in (1, 3, 2):
-        go(kv_copy(kvb.at[h], h, x, e, z * XS + (x + e) % XS))
-    kvr[h, x] = kvb[h]
+        return remote(src, kvr.at[row, col], kv_send.at[slot], kv_recv.at[row * XS + col], dev)
+
+    def kv_first(i):
+        zd = spot(outer // 2, H * c + i)
+        stays = jnp.logical_and(zd == z, outer % 2 == c)
+        return stays, kv_copy(kvb.at[i], z // (Z // 2), x, i, (zd * XS + x, 2 * y + outer % 2))
+
+    for i in range(H):
+        stays, copy = kv_first(i)
+
+        @pl.when(stays)
+        def _():
+            kvr[z // (Z // 2), x] = kvb[i]
+
+        @pl.when(jnp.logical_not(stays))
+        def _():
+            copy.start()
 
     queries = jnp.dot(rows_all, wq[...], preferred_element_type=f32) * (dh ** (-0.5) * log2e)
     q_turned = queries.T.astype(bf16)
     for i in range(H):
         qb[i] = q_turned[i * dh : (i + 1) * dh]
-    qr[z] = qb[h]
-
-    def q_copy(i, depth):
-        dev = depth if i == 0 else Z - 1 - depth
-        return dev, remote(qb.at[i], qr.at[z], q_send.at[i * half_z + depth], q_recv.at[z], (dev * XS + x, t))
+
+    def q_first(i, group):
+        zd = spot(group, H * c + i)
+        stays = jnp.logical_and(zd == z, c == 0)
+        copy = remote(qb.at[i], qr.at[z], q_send.at[i * 2 + group], q_recv.at[z], (zd * XS + x, 2 * y))
+        return stays, z >= 2 * group, copy
 
     def q_extra(i):
-        dev = mz if i == 0 else z
-        return remote(qb.at[i], qr.at[Z], q_send.at[H * half_z + i], q_recv.at[Z], (dev * XS + XS - 1 - x, t))
+        depth = Z - 1 - z
+        zd = spot(depth // 2, H * c + i)
+        dev = (zd * XS + XS - 1 - x, 2 * y + depth % 2)
+        return remote(qb.at[i], qr.at[Z], q_send.at[2 * H + i], q_recv.at[Z], dev)
 
     def each_q(act_on):
-        @pl.when(h == 1)
+        for group in (0, 1):
+            for i in range(H):
+                stays, wanted, copy = q_first(i, group)
+
+                @pl.when(jnp.logical_and(wanted, jnp.logical_not(stays)))
+                def _():
+                    act_on(copy)
+
+        @pl.when(z >= Z // 2)
         def _():
             for i in range(H):
                 act_on(q_extra(i))
 
-        for depth in range(half_z - 1, -1, -1):
-            for i in range(H):
-                dev, copy = q_copy(i, depth)
-
-                @pl.when(jnp.logical_and(depth <= z, dev != z))
-                def _():
-                    act_on(copy)
+    for i in range(H):
+        for group in (0, 1):
+            stays, wanted, _ = q_first(i, group)
+
+            @pl.when(jnp.logical_and(wanted, stays))
+            def _():
+                qr[z] = qb[i]
 
     each_q(lambda copy: copy.start())
 
     def kv_wait(row, col):
-        @pl.when(jnp.logical_or(row != h, col != x))
-        def _():
-            remote(kvb.at[0], kvr.at[row, col], kv_send.at[0], kv_recv.at[row * XS + col], (s, t)).wait_recv()
+        remote(kvb.at[0], kvr.at[row, col], kv_send.at[0], kv_recv.at[row * XS + col], (s, t)).wait_recv()
+
+    def q_forward(slot):
+        return remote(qr.at[slot], qr.at[slot], f_send.at[slot], q_recv.at[slot], (s, partner))
 
     def q_wait(slot):
-        @pl.when(slot != z)
-        def _():
-            remote(qb.at[0], qr.at[slot], q_send.at[0], q_recv.at[slot], (s, t)).wait_recv()
+        local = jnp.logical_and(jnp.logical_and(slot == z, c == 0), hl // H == 0)
+
+        @pl.when(jnp.logical_not(local))
+        def _():
+            q_forward(slot).wait_recv()
+
+    x_on = (x + 1 + (XS - 2) * c) % XS
+    x_back = (x + XS - 1 - (XS - 2) * c) % XS
+    x_far = (x + 2) % XS
+
+    def kv_spread(row):
+        base = H + row * 3
+        return (
+            kv_copy(kvr.at[row, x], row, x, base, (z * XS + x_on, t)),
+            kv_copy(kvr.at[row, x], row, x, base + 1, (z * XS + x_back, t)),
+            kv_copy(kvr.at[row, x_back], row, x_back, base + 2, (z * XS + x_on, t)),
+        )
+
+    for row in range(2):
+        local = jnp.logical_and(z == (kz if row == 0 else Z - 1 - kz), home)
+
+        @pl.when(jnp.logical_not(local))
+        def _():
+            kv_wait(row, x)
+
+        for copy in kv_spread(row)[:2]:
+            copy.start()
+
+    kv_wait(0, x_back)
+    kv_spread(0)[2].start()
+
+    theirs = offs.at[pl.ds(H * (1 - c), H)]
+    remote(theirs, theirs, off_send.at[0], off_recv.at[0], (s, partner)).wait_recv()
+    whole = jnp.concatenate([jnp.broadcast_to(offs[hl], (16, 128))] * (B // 128), axis=1)
+    high = whole.astype(bf16).astype(f32)
+    middle = (whole - high).astype(bf16).astype(f32)
+    low = whole - high - middle
+    part_row = lax.broadcasted_iota(jnp.int32, (16, B), 0)
+    offt[...] = jnp.where(
+        part_row == 0, high, jnp.where(part_row == 1, middle, jnp.where(part_row == 2, low, 0.0))
+    ).astype(bf16)
 
     lane = lax.broadcasted_iota(jnp.int32, (16, 128), 1)
     ones = (lane < 3).astype(f32).astype(bf16)
@@ -279,19 +354,13 @@
         part = jnp.dot(vt, weight, preferred_element_type=f32)
         acc[:, sl] = part if first else acc[:, sl] * total + part
 
-    def unit_of(turn):
-        j = jnp.where(h == 0, turn, Z - 2 - turn)
-        is_low = j < Z - 1 - kz
-        zq = jnp.where(is_low, kz + 1 + j, j + 1)
-        return jnp.where(is_low, 0, 1), zq
-
     def o_copies(u, r, e, dst, dev):
         return (
             remote(obuf.at[u, r], orecv.at[dst], o_send.at[u * T + e], o_recv.at[dst], dev),
             remote(tbuf.at[u, r], trecv.at[dst], t_send.at[u * T + e], t_recv.at[dst], dev),
         )
 
-    def send_out(u, row, block, kept):
+    def send_out(u, slot, block, kept):
         lanes = lax.broadcasted_iota(jnp.int32, (dh // 2, 128), 1) < dh
         lanes_t = lax.broadcasted_iota(jnp.int32, (8, 128), 1) < dh
         for g in range(T // 2):
@@ -306,7 +375,7 @@
                 fac = jnp.where(lanes_t, tr, tt) if odd else jnp.where(lanes_t, tt, tr)
                 obuf[u, 2 * g + odd] = body.astype(bf16)
                 tbuf[u, 2 * g + odd] = fac[:1]
-        dst = row * T * H + t * H + h
+        dst = slot * T * H + head
         for e in range(1, T):
             r = (t + e) % T
             for copy in o_copies(u, r, e, dst, (block, r)):
@@ -322,94 +391,119 @@
             orecv[dst] = obuf[u, t]
             trecv[dst] = tbuf[u, t]
 
-    def key_row(row):
-        return jnp.where(row == 0, kz, Z - 1 - kz)
-
-    def self_unit(u, row, fresh):
-        n = jnp.where(row == 0, x, XS - 1 - x)
-        slot = jnp.where(row == 0, kz, Z)
+    def merge(slot, kept):
+        remote(mbuf.at[slot], mbuf.at[slot], m_send.at[slot], m_recv.at[slot], (s, t)).wait_recv()
+        out_kept = []
+        for j in range(2):
+            sl = slice(j * W, (j + 1) * W)
+            acc[:, sl] = mbuf[slot, :dh, sl] * kept[j] + acc[:, sl]
+            out_kept.append(mbuf[slot, dh : dh + 1, sl] * kept[j])
+        return out_kept
+
+    def self_unit(row):
+        n = x if row == 0 else XS - 1 - x
+        zq = kz if row == 0 else Z - 1 - kz
+        slot = kz if row == 0 else Z
         q_wait(slot)
         for j in range(2):
             acc[:, j * W : (j + 1) * W] = jnp.zeros((dh, W), f32)
 
         def step(col, kept):
-            if fresh:
-                kv_wait(row, col)
-            nxt = []
-            found = []
-            for j in range(2):
-                found.append(weigh(row, col, slot, j, False))
+            found = [weigh(row, col, slot, j, False) for j in range(2)]
             for j in range(2):
                 gather(row, col, j, *found[j], False)
-                nxt.append(kept[j] * found[j][1])
-            return tuple(nxt)
+            return tuple(kept[j] * found[j][1] for j in range(2))
 
         one = jnp.ones((1, W), f32)
         kept = lax.fori_loop(0, n, step, (one, one))
-        if fresh:
-            kv_wait(row, n)
         found = [weigh(row, n, slot, j, True) for j in range(2)]
         for j in range(2):
             gather(row, n, j, *found[j], False)
-        send_out(u, key_row(row), key_row(row) * XS + n, [kept[j] * found[j][1] for j in range(2)])
-        return n
-
-    n = self_unit(0, h, True)
-    for col in range(XS):
-
-        @pl.when(col > n)
-        def _():
-            kv_wait(h, col)
-
-    kv_wait(1 - h, x)
-    for e in (1, 3, 2):
-        go(kv_copy(kvr.at[1 - h, x], 1 - h, x, 3 + e, z * XS + (x + e) % XS))
-
-    turn_over = jnp.where(h == 0, Z - 1 - kz, kz)
-
-    def mirrored():
-        for e in range(1, XS):
-            kv_wait(1 - h, (x + e) % XS)
+        kept = [kept[j] * found[j][1] for j in range(2)]
+        if row == 0:
+
+            @pl.when(c == 0)
+            def _():
+                send_out(kz, g, zq * XS + n, kept)
+
+            @pl.when(c == 1)
+            def _():
+                send_out(kz, g, zq * XS + n, merge(kz, kept))
+        else:
+            send_out(LAST, Z - 3 - kz, zq * XS + n, kept)
 
     def full(turn, unused):
-        row, zq = unit_of(turn)
-
-        @pl.when(turn == turn_over)
-        def _():
-            mirrored()
-
-        later_use = jnp.logical_and(row != h, zq > Z - 1 - kz)
-
-        @pl.when(jnp.logical_not(later_use))
-        def _():
-            q_wait(zq)
-
-        kept = [None, None]
-        waiting = None
-        for col in range(XS):
+        low_row = turn < Z
+        hop = (turn + 1) // 2
+        near = jnp.where(turn % 2 == 1, z + hop, z + Z - hop) % Z
+        zq = jnp.where(low_row, near, turn - Z)
+        row = jnp.where(low_row, 0, 1)
+        valid = jnp.where(low_row, zq - kz > 0, zq + kz >= Z)
+
+        @pl.when(turn == 2)
+        def _():
+            kv_wait(1, x_back)
+            kv_spread(1)[2].start()
+
+        @pl.when(turn == Z)
+        def _():
+            kv_wait(1, x_on)
+            kv_wait(1, x_far)
+
+        @pl.when(valid)
+        def _():
+            @pl.when(low_row)
+            def _():
+                q_wait(zq)
+
+                @pl.when(c == 0)
+                def _():
+                    q_forward(zq).start()
+
+            kept = [None, None]
+            waiting = None
+            for col in range(XS):
+                for j in range(2):
+                    later, total = weigh(row, col, zq, j, False)
+                    if waiting is not None:
+                        gather(*waiting)
+                    waiting = (row, col, j, later, total, col == 0)
+                    kept[j] = total if col == 0 else kept[j] * total
+            gather(*waiting)
             for j in range(2):
-                later, total = weigh(row, col, zq, j, False)
-                if waiting is not None:
-                    gather(*waiting)
-                waiting = (row, col, j, later, total, col == 0)
-                kept[j] = total if col == 0 else kept[j] * total
-        gather(*waiting)
-        send_out(turn + 1, key_row(row), zq * XS + x, kept)
+                factors[:, j * W : (j + 1) * W] = jnp.broadcast_to(kept[j], (8, W))
+
+            handed = jnp.logical_and(low_row, c == 0)
+
+            @pl.when(handed)
+            def _():
+                mbuf[zq, :dh] = acc[...]
+                mbuf[zq, dh:] = factors[...]
+                remote(mbuf.at[zq], mbuf.at[zq], m_send.at[zq], m_recv.at[zq], (s, partner)).start()
+
+            @pl.when(jnp.logical_and(low_row, c == 1))
+            def _():
+                for j, both in enumerate(merge(zq, kept)):
+                    factors[:, j * W : (j + 1) * W] = jnp.broadcast_to(both, (8, W))
+
+            @pl.when(jnp.logical_not(handed))
+            def _():
+                u = jnp.where(low_row, zq, zq + 3)
+                slot = jnp.where(low_row, g, Z - 3 - kz)
+                send_out(u, slot, zq * XS + x, [factors[:1, j * W : (j + 1) * W] for j in range(2)])
+
         return unused
 
-    lax.fori_loop(0, 3, full, 0)
     go(w_copy(wrow(t), t, 0, partner))
     for e in range(1, Y):
         came = ((y + e) % Y) * 2 + c
         w_copy(wrow(t), came, 0, partner).wait_recv()
         go(w_copy(wrow(came), came, Y + e - 1, partner))
-    lax.fori_loop(3, Z - 1, full, 0)
-
-    @pl.when(turn_over == Z - 1)
-    def _():
-        mirrored()
-
-    self_unit(Z, 1 - h, False)
+    kv_wait(0, x_on)
+    kv_wait(0, x_far)
+    lax.fori_loop(0, 2 * Z, full, 0)
+    self_unit(0)
+    self_unit(1)
 
     w_copy(wrow(t), partner, 0, partner).wait_recv()
     for e in range(1, Y):
@@ -418,10 +512,15 @@
     for hh in range(T * H):
         heads[hh] = jnp.zeros((dh // 2, 128), f32)
 
+    def made_here(slot):
+        low_made = jnp.where(c == 1, z >= kz, z == kz)
+        high_made = jnp.logical_and(slot == Z - 3 - kz, z + kz >= Z)
+        return jnp.logical_or(jnp.logical_and(slot == g, low_made), high_made)
+
     def combine(r, unused):
         for hh in range(T * H):
 
-            @pl.when(jnp.logical_or(r != kz, hh != t * H + h))
+            @pl.when(jnp.logical_not(jnp.logical_and(hh == head, made_here(r))))
             def _():
                 e = r * T * H + hh
                 for copy in o_copies(0, 0, 0, e, (s, t)):
@@ -431,7 +530,8 @@
             heads[hh] = heads[hh] * trecv[r * T * H + hh] + orecv[r * T * H + hh].astype(f32)
         return unused
 
-    lax.fori_loop(0, z + 1, combine, 0)
+    slots = jnp.where(z < 2, 1, jnp.where(z < 4, 2, z - 1))
+    lax.fori_loop(0, slots, combine, 0)
 
     lhs, rhs = [], []
     for q in range(T * H // 4):
@@ -450,27 +550,46 @@
         copy.wait_send()
     each_q(lambda copy: copy.wait_send())
 
-    def sent(u, block):
-        for e in range(1, T):
-            for copy in o_copies(u, 0, e, 0, (s, t)):
-                copy.wait_send()
-
-        @pl.when(block != s)
-        def _():
-            for copy in o_copies(u, 0, 0, 0, (s, t)):
-                copy.wait_send()
-
-    def self_block(row):
-        return key_row(row) * XS + jnp.where(row == 0, x, XS - 1 - x)
-
-    sent(0, self_block(h))
-    sent(Z, self_block(1 - h))
-
-    def sent_full(turn, unused):
-        sent(turn + 1, unit_of(turn)[1] * XS + x)
+    for i in range(H):
+        stays, copy = kv_first(i)
+
+        @pl.when(jnp.logical_not(stays))
+        def _():
+            copy.wait_send()
+
+    for row in range(2):
+        for copy in kv_spread(row):
+            copy.wait_send()
+
+    def sent(u, valid, block):
+        @pl.when(valid)
+        def _():
+            for e in range(1, T):
+                for copy in o_copies(u, 0, e, 0, (s, t)):
+                    copy.wait_send()
+
+            @pl.when(block != s)
+            def _():
+                for copy in o_copies(u, 0, 0, 0, (s, t)):
+                    copy.wait_send()
+
+    def sent_low(zq, unused):
+        sent(zq, jnp.logical_or(zq == kz, jnp.logical_and(zq > kz, c == 1)), zq * XS + x)
+
+        @pl.when(jnp.logical_and(zq > kz, c == 0))
+        def _():
+            q_forward(zq).wait_send()
+            remote(mbuf.at[zq], mbuf.at[zq], m_send.at[zq], m_recv.at[zq], (s, partner)).wait_send()
+
         return unused
 
-    lax.fori_loop(0, Z - 1, sent_full, 0)
+    def sent_high(zq, unused):
+        sent(zq + 3, zq + kz >= Z, zq * XS + x)
+        return unused
+
+    lax.fori_loop(0, Z, sent_low, 0)
+    lax.fori_loop(5, Z, sent_high, 0)
+    sent(LAST, z >= 0, (Z - 1 - kz) * XS + XS - 1 - x)
 
 
 def solution(mesh):
@@ -508,10 +627,13 @@
                 pltpu.VMEM((16, B), bf16),
                 pltpu.VMEM((2, B, B // 2), bf16),
                 pltpu.VMEM((dh, B), f32),
-                pltpu.VMEM((Z + 1, T, dh // 2, 128), bf16),
-                pltpu.VMEM((Z * T * H, dh // 2, 128), bf16),
-                pltpu.VMEM((Z + 1, T, 1, 128), f32),
-                pltpu.VMEM((Z * T * H, 1, 128), f32),
+                pltpu.VMEM((8, B), f32),
+                pltpu.VMEM((Z, dh + 8, B), f32),
+                pltpu.VMEM((2 * H, 1, 128), f32),
+                pltpu.VMEM((LAST + 1, T, dh // 2, 128), bf16),
+                pltpu.VMEM((6 * T * H, dh // 2, 128), bf16),
+                pltpu.VMEM((LAST + 1, T, 1, 128), f32),
+                pltpu.VMEM((6 * T * H, 1, 128), f32),
                 pltpu.VMEM((T * H, dh // 2, 128), f32),
                 dma((T,)),
                 dma((T,)),
@@ -519,12 +641,17 @@
                 dma((T,)),
                 dma((8,)),
                 dma((2 * XS,)),
-                dma((H * Z // 2 + H,)),
+                dma((3 * H,)),
                 dma((Z + 1,)),
-                dma(((Z + 1) * T,)),
-                dma((Z * T * H,)),
-                dma(((Z + 1) * T,)),
-                dma((Z * T * H,)),
+                dma((Z + 1,)),
+                dma((Z,)),
+                dma((Z,)),
+                dma((1,)),
+                dma((1,)),
+                dma(((LAST + 1) * T,)),
+                dma((6 * T * H,)),
+                dma(((LAST + 1) * T,)),
+                dma((6 * T * H,)),
                 dma((7,)),
             ],
             compiler_params=pltpu.CompilerParams(collective_id=0, has_side_effects=True, vmem_limit_bytes=67043328),

time: 78.1 us -> 74.9 us (0.959)
  the two profiles are of different devices: /device:TPU:225 before, /device:TPU:1 now
where the time goes in v3:
time: 74.9 us; the launch traced here: 74.8 us
  Pallas kernels  73.2 us (98%)
  local copies, waits for them, and re-layouts  1.57 us (2%)
    pallas_call x1, Pallas kernels, local(): pl.pallas_call(functools.partial(layer_kernel, S, T, H, dh), out_shape=ja...  73.2 us
    unnamed x1, local copies, waits for them, and re-layouts  1.57 us

profile of v3, /device:TPU:1, one launch (start us, length us, event | category | flops | bytes accessed | tf_op | source)
XLA Modules:
  0.0 74.8 jit_solution(6646655899652266411)
XLA Ops:
  0.0 73.2 %shard_map.82 = bf16[64,1024]{1,0:T(8,128)(2,1)} custom-call(bf16[64,1024]{1,0:T(8,128)(2,1)} %act_hbm.1, f32[1,1024]{1,0:T(1,128)} %bitcast.2, bf16[1024,128]{1,0:T(8,128)(2,1)} %wq_hbm.1, bf16[1024,128]{1,0:T(8,128)(2,1)} %wk_hbm.1, bf16[1024,128]{1,0:T(8,128)(2,1)} %wv_hbm.1, f32[2]{0:T(128)} %off.1, bf16[128,1024]{1,0:T(8,128)(2,1)} %wo_hbm.1, ...), custom_call_target="tpu_custom_call" | custom-call | tf_op jit(solution)/shard_map/pallas_call | solution.py:608
  73.2 1.6 %copy.10 = bf16[64,1024]{1,0:T(8,128)(2,1)} copy(bf16[64,1024]{1,0:T(8,128)(2,1)} %shard_map.82) | data formatting | bytes 262144

commit v4 on v3

--- a/solution.py
+++ b/solution.py
@@ -162,7 +162,7 @@
 
     token = lax.broadcasted_iota(jnp.int32, (B, B), 0)
     place = lax.broadcasted_iota(jnp.int32, (B, B), 1)
-    perm[...] = (token == (place & (T - 1)) * R + (place >> (T.bit_length() - 1))).astype(f32).astype(bf16)
+    perm[...] = (token == (place & (T - 1)) * R + R - 1 - (place >> (T.bit_length() - 1))).astype(f32).astype(bf16)
     for i in range(H):
         offs[H * c + i] = jnp.broadcast_to(off[i] * log2e, (1, 128)).astype(f32)
     mine = offs.at[pl.ds(H * c, H)]
@@ -197,8 +197,30 @@
 
     outer = jnp.minimum(z, Z - 1 - z)
 
+    class Both:
+        def __init__(self, parts):
+            self.parts = parts
+
+        def start(self):
+            for part in self.parts:
+                part.start()
+
+        def wait_send(self):
+            for part in self.parts:
+                part.wait_send()
+
+    def kv_part(src, row, col, slot, dev, part):
+        rows_of = pl.ds(part * W, W)
+        return remote(
+            src.at[rows_of],
+            kvr.at[row, col, rows_of],
+            kv_send.at[2 * slot + part],
+            kv_recv.at[2 * (row * XS + col) + part],
+            dev,
+        )
+
     def kv_copy(src, row, col, slot, dev):
-        return remote(src, kvr.at[row, col], kv_send.at[slot], kv_recv.at[row * XS + col], dev)
+        return Both([kv_part(src, row, col, slot, dev, part) for part in range(2)])
 
     def kv_first(i):
         zd = spot(outer // 2, H * c + i)
@@ -255,10 +277,10 @@
             def _():
                 qr[z] = qb[i]
 
-    each_q(lambda copy: copy.start())
 
     def kv_wait(row, col):
-        remote(kvb.at[0], kvr.at[row, col], kv_send.at[0], kv_recv.at[row * XS + col], (s, t)).wait_recv()
+        for part in range(2):
+            kv_part(kvb.at[0], row, col, 0, (s, t), part).wait_recv()
 
     def q_forward(slot):
         return remote(qr.at[slot], qr.at[slot], f_send.at[slot], q_recv.at[slot], (s, partner))
@@ -285,15 +307,19 @@
     for row in range(2):
         local = jnp.logical_and(z == (kz if row == 0 else Z - 1 - kz), home)
 
-        @pl.when(jnp.logical_not(local))
-        def _():
-            kv_wait(row, x)
-
-        for copy in kv_spread(row)[:2]:
-            copy.start()
-
-    kv_wait(0, x_back)
-    kv_spread(0)[2].start()
+        for part in range(2):
+
+            @pl.when(jnp.logical_not(local))
+            def _():
+                kv_part(kvb.at[0], row, x, 0, (s, t), part).wait_recv()
+
+            for copy in kv_spread(row)[:2]:
+                copy.parts[part].start()
+
+    each_q(lambda copy: copy.start())
+    for part in range(2):
+        kv_part(kvb.at[0], 0, x_back, 0, (s, t), part).wait_recv()
+        kv_spread(0)[2].parts[part].start()
 
     theirs = offs.at[pl.ds(H * (1 - c), H)]
     remote(theirs, theirs, off_send.at[0], off_recv.at[0], (s, partner)).wait_recv()
@@ -321,22 +347,24 @@
                 - R * lax.broadcasted_iota(jnp.int32, (8, W), 0)
             )
         lhs = jnp.concatenate([kvr[row, col, :W], jnp.tile(ones, (W // 16, 1))], axis=1)
-        for part in (1, 0):
+        for part in (0, 1):
             q = qr[slot, :, sl]
             stack = [q, zeros] if part == 0 else [zeros, q]
             rhs = jnp.concatenate(stack + [offt[:, sl], pad], axis=0)
-            score = jnp.minimum(jnp.dot(lhs, rhs, preferred_element_type=f32), ZMAX)
-            for v in range(W // 8 - 2, -1, -2):
-                e0 = jnp.exp2(score[8 * v : 8 * v + 8])
-                e1 = jnp.exp2(score[8 * v + 8 : 8 * v + 16])
+            for v in range(0, W // 8, 2):
+                if v % 8 == 0:
+                    chunk = jnp.dot(lhs[8 * v : 8 * v + 64], rhs, preferred_element_type=f32)
+                    score = [None] * v + [jnp.minimum(chunk[8 * w : 8 * w + 8], ZMAX) for w in range(8)]
+                e0 = jnp.exp2(score[v])
+                e1 = jnp.exp2(score[v + 1])
                 if masked:
                     place_v = part * (W // 8) + v
-                    e0 = jnp.where(ahead > place_v, e0, 0.0)
-                    e1 = jnp.where(ahead > place_v + 1, e1, 0.0)
+                    e0 = jnp.where(ahead > R - 1 - place_v, e0, 0.0)
+                    e1 = jnp.where(ahead > R - 2 - place_v, e1, 0.0)
                 u0, u1 = 1.0 + e0, 1.0 + e1
                 left = run * (1.0 / (u0 * u1))
-                first = e0 * left
-                second = e1 * (u0 * left)
+                first = e0 * (u1 * left)
+                second = e1 * left
                 run = left
                 base = part * W + 8 * v
                 ws[j, base : base + 16] = jnp.concatenate([first, second], axis=0).astype(bf16)
@@ -434,8 +462,9 @@
 
     def full(turn, unused):
         low_row = turn < Z
-        hop = (turn + 1) // 2
-        near = jnp.where(turn % 2 == 1, z + hop, z + Z - hop) % Z
+        far = Z - 1 - turn
+        hop = (far + 1) // 2
+        near = jnp.where(far % 2 == 1, z + hop, z + 2 * Z - hop) % Z
         zq = jnp.where(low_row, near, turn - Z)
         row = jnp.where(low_row, 0, 1)
         valid = jnp.where(low_row, zq - kz > 0, zq + kz >= Z)
@@ -639,8 +668,8 @@
                 dma((T,)),
                 dma((T,)),
                 dma((T,)),
-                dma((8,)),
-                dma((2 * XS,)),
+                dma((16,)),
+                dma((4 * XS,)),
                 dma((3 * H,)),
                 dma((Z + 1,)),
                 dma((Z + 1,)),

time: 74.9 us -> 71.7 us (0.957)
  Pallas kernels: 73.2 us -> 70 us
    pallas_call x1, Pallas kernels: 73.2 us -> 70 us  [local(): pl.pallas_call(functools.partial(layer_kernel, S, T, H, dh), out_shape=ja...]
where the time goes in v4:
time: 71.7 us; the launch traced here: 71.6 us
  Pallas kernels  70 us (98%)
  local copies, waits for them, and re-layouts  1.57 us (2%)
    pallas_call x1, Pallas kernels, local(): pl.pallas_call(functools.partial(layer_kernel, S, T, H, dh), out_shape=ja...  70 us
    unnamed x1, local copies, waits for them, and re-layouts  1.57 us

profile of v4, /device:TPU:1, one launch (start us, length us, event | category | flops | bytes accessed | tf_op | source)
XLA Modules:
  0.0 71.6 jit_solution(8398609077911630170)
XLA Ops:
  0.0 70.0 %shard_map.82 = bf16[64,1024]{1,0:T(8,128)(2,1)} custom-call(bf16[64,1024]{1,0:T(8,128)(2,1)} %act_hbm.1, f32[1,1024]{1,0:T(1,128)} %bitcast.2, bf16[1024,128]{1,0:T(8,128)(2,1)} %wq_hbm.1, bf16[1024,128]{1,0:T(8,128)(2,1)} %wk_hbm.1, bf16[1024,128]{1,0:T(8,128)(2,1)} %wv_hbm.1, f32[2]{0:T(128)} %off.1, bf16[128,1024]{1,0:T(8,128)(2,1)} %wo_hbm.1, ...), custom_call_target="tpu_custom_call" | custom-call | tf_op jit(solution)/shard_map/pallas_call | solution.py:637
  70.0 1.6 %copy.10 = bf16[64,1024]{1,0:T(8,128)(2,1)} copy(bf16[64,1024]{1,0:T(8,128)(2,1)} %shard_map.82) | data formatting | bytes 262144

commit v5 on v4

--- a/solution.py
+++ b/solution.py
@@ -15,6 +15,8 @@
 XS = 4
 ZMAX = 63.0
 LAST = 11
+FIRST = 5
+SELF_TURN = 9
 
 
 def scaled_rows(widened, row_gain):
@@ -52,13 +54,12 @@
     offt,
     ws,
     acc,
+    duo,
     factors,
     mbuf,
     offs,
     obuf,
     orecv,
-    tbuf,
-    trecv,
     heads,
     x_send,
     x_recv,
@@ -75,8 +76,6 @@
     off_recv,
     o_send,
     o_recv,
-    t_send,
-    t_recv,
     load,
 ):
     R = act.shape[0]
@@ -292,6 +291,13 @@
         def _():
             q_forward(slot).wait_recv()
 
+    def q_get(slot):
+        q_wait(slot)
+
+        @pl.when(c == 0)
+        def _():
+            q_forward(slot).start()
+
     x_on = (x + 1 + (XS - 2) * c) % XS
     x_back = (x + XS - 1 - (XS - 2) * c) % XS
     x_far = (x + 2) % XS
@@ -304,9 +310,8 @@
             kv_copy(kvr.at[row, x_back], row, x_back, base + 2, (z * XS + x_on, t)),
         )
 
-    for row in range(2):
+    def kv_relay(row):
         local = jnp.logical_and(z == (kz if row == 0 else Z - 1 - kz), home)
-
         for part in range(2):
 
             @pl.when(jnp.logical_not(local))
@@ -316,10 +321,12 @@
             for copy in kv_spread(row)[:2]:
                 copy.parts[part].start()
 
+    kv_relay(0)
     each_q(lambda copy: copy.start())
     for part in range(2):
         kv_part(kvb.at[0], 0, x_back, 0, (s, t), part).wait_recv()
         kv_spread(0)[2].parts[part].start()
+    kv_relay(1)
 
     theirs = offs.at[pl.ds(H * (1 - c), H)]
     remote(theirs, theirs, off_send.at[0], off_recv.at[0], (s, partner)).wait_recv()
@@ -380,16 +387,19 @@
         weight = (ws[j].reshape(B // 16, 16, W) * later[None]).reshape(B, W)
         vt = jnp.concatenate([kvr[row, col, W + p * dh : W + (p + 1) * dh] for p in range(4)], axis=1)
         part = jnp.dot(vt, weight, preferred_element_type=f32)
-        acc[:, sl] = part if first else acc[:, sl] * total + part
+        if first is None:
+            duo[row, :, sl] = duo[row, :, sl] * total + part
+        else:
+            acc[:, sl] = part if first else acc[:, sl] * total + part
 
     def o_copies(u, r, e, dst, dev):
         return (
             remote(obuf.at[u, r], orecv.at[dst], o_send.at[u * T + e], o_recv.at[dst], dev),
-            remote(tbuf.at[u, r], trecv.at[dst], t_send.at[u * T + e], t_recv.at[dst], dev),
         )
 
     def send_out(u, slot, block, kept):
         lanes = lax.broadcasted_iota(jnp.int32, (dh // 2, 128), 1) < dh
+        top = lax.broadcasted_iota(jnp.int32, (8, 128), 0) == 0
         lanes_t = lax.broadcasted_iota(jnp.int32, (8, 128), 1) < dh
         for g in range(T // 2):
             cols = slice(g * 128, (g + 1) * 128)
@@ -401,8 +411,9 @@
             for odd in range(2):
                 body = jnp.where(lanes, ar, b) if odd else jnp.where(lanes, a, br)
                 fac = jnp.where(lanes_t, tr, tt) if odd else jnp.where(lanes_t, tt, tr)
-                obuf[u, 2 * g + odd] = body.astype(bf16)
-                tbuf[u, 2 * g + odd] = fac[:1]
+                fac_high = fac.astype(bf16).astype(f32)
+                tail = jnp.where(top, fac_high, fac - fac_high)
+                obuf[u, 2 * g + odd] = jnp.concatenate([body, tail], axis=0).astype(bf16)
         dst = slot * T * H + head
         for e in range(1, T):
             r = (t + e) % T
@@ -417,7 +428,6 @@
         @pl.when(block == s)
         def _():
             orecv[dst] = obuf[u, t]
-            trecv[dst] = tbuf[u, t]
 
     def merge(slot, kept):
         remote(mbuf.at[slot], mbuf.at[slot], m_send.at[slot], m_recv.at[slot], (s, t)).wait_recv()
@@ -428,66 +438,84 @@
             out_kept.append(mbuf[slot, dh : dh + 1, sl] * kept[j])
         return out_kept
 
-    def self_unit(row):
-        n = x if row == 0 else XS - 1 - x
-        zq = kz if row == 0 else Z - 1 - kz
-        slot = kz if row == 0 else Z
-        q_wait(slot)
-        for j in range(2):
-            acc[:, j * W : (j + 1) * W] = jnp.zeros((dh, W), f32)
-
-        def step(col, kept):
-            found = [weigh(row, col, slot, j, False) for j in range(2)]
+    def self_units():
+        slots = (kz, Z)
+        q_wait(slots[0])
+        q_wait(slots[1])
+        ends = (x, XS - 1 - x)
+        duo[...] = jnp.zeros((2, dh, B), f32)
+        one = jnp.ones((1, W), f32)
+        kept = [[one, one], [one, one]]
+        waiting = None
+        for p in range(XS + 1):
+            if p < XS - 1:
+                row = jnp.where(p < x, 0, 1)
+                col = jnp.where(p < x, p, p - x)
+                slot = jnp.where(p < x, kz, Z)
+            else:
+                row = p - XS + 1
+                col, slot = ends[row], slots[row]
             for j in range(2):
-                gather(row, col, j, *found[j], False)
-            return tuple(kept[j] * found[j][1] for j in range(2))
-
-        one = jnp.ones((1, W), f32)
-        kept = lax.fori_loop(0, n, step, (one, one))
-        found = [weigh(row, n, slot, j, True) for j in range(2)]
-        for j in range(2):
-            gather(row, n, j, *found[j], False)
-        kept = [kept[j] * found[j][1] for j in range(2)]
-        if row == 0:
-
-            @pl.when(c == 0)
-            def _():
-                send_out(kz, g, zq * XS + n, kept)
-
-            @pl.when(c == 1)
-            def _():
-                send_out(kz, g, zq * XS + n, merge(kz, kept))
-        else:
-            send_out(LAST, Z - 3 - kz, zq * XS + n, kept)
+                later, total = weigh(row, col, slot, j, p >= XS - 1)
+                if waiting is not None:
+                    gather(*waiting)
+                waiting = (row, col, j, later, total, None)
+                for k in range(2):
+                    kept[k][j] = kept[k][j] * (jnp.where(row == k, total, 1.0) if p < XS - 1 else total if row == k else one)
+        gather(*waiting)
+
+        acc[...] = duo[0]
+
+        @pl.when(c == 0)
+        def _():
+            send_out(kz, g, kz * XS + x, kept[0])
+
+        @pl.when(c == 1)
+        def _():
+            send_out(kz, g, kz * XS + x, merge(kz, kept[0]))
+
+        acc[...] = duo[1]
+        send_out(LAST, Z - 3 - kz, (Z - 1 - kz) * XS + XS - 1 - x, kept[1])
 
     def full(turn, unused):
-        low_row = turn < Z
-        far = Z - 1 - turn
+        low_row = jnp.logical_or(turn <= FIRST, turn > FIRST + 3)
+        far = jnp.where(turn < FIRST, Z - 1 - turn, Z + 3 - turn)
         hop = (far + 1) // 2
         near = jnp.where(far % 2 == 1, z + hop, z + 2 * Z - hop) % Z
-        zq = jnp.where(low_row, near, turn - Z)
+        shared = 2 * g + 1
+        zq = jnp.where(turn == FIRST, shared, jnp.where(low_row, near, Z + FIRST - turn))
         row = jnp.where(low_row, 0, 1)
-        valid = jnp.where(low_row, zq - kz > 0, zq + kz >= Z)
-
-        @pl.when(turn == 2)
+        low_valid = jnp.where(turn == FIRST, c == 0, zq > shared)
+        valid = jnp.where(low_row, low_valid, zq + kz >= Z)
+
+        @pl.when(turn == 1)
         def _():
             kv_wait(1, x_back)
             kv_spread(1)[2].start()
 
-        @pl.when(turn == Z)
+        @pl.when(turn == FIRST)
+        def _():
+            for step in (0, 1, Z - 1):
+                close = (z + step) % Z
+
+                @pl.when(close >= Z - 1 - 2 * g)
+                def _():
+                    q_get(close)
+
+        @pl.when(turn == FIRST + 1)
         def _():
             kv_wait(1, x_on)
             kv_wait(1, x_far)
 
+        @pl.when(turn == SELF_TURN)
+        def _():
+            self_units()
+
         @pl.when(valid)
         def _():
-            @pl.when(low_row)
+            @pl.when(jnp.logical_and(low_row, jnp.logical_or(turn <= FIRST, zq < Z - 1 - 2 * g)))
             def _():
-                q_wait(zq)
-
-                @pl.when(c == 0)
-                def _():
-                    q_forward(zq).start()
+                q_get(zq)
 
             kept = [None, None]
             waiting = None
@@ -530,10 +558,7 @@
         go(w_copy(wrow(came), came, Y + e - 1, partner))
     kv_wait(0, x_on)
     kv_wait(0, x_far)
-    lax.fori_loop(0, 2 * Z, full, 0)
-    self_unit(0)
-    self_unit(1)
-
+    lax.fori_loop(0, Z + 4, full, 0)
     w_copy(wrow(t), partner, 0, partner).wait_recv()
     for e in range(1, Y):
         w_copy(wrow(t), ((y + e) % Y) * 2 + 1 - c, 0, partner).wait_recv()
@@ -556,7 +581,9 @@
                     copy.wait_recv()
 
         for hh in range(T * H):
-            heads[hh] = heads[hh] * trecv[r * T * H + hh] + orecv[r * T * H + hh].astype(f32)
+            got = orecv[r * T * H + hh].astype(f32)
+            fac = got[dh // 2 : dh // 2 + 1] + got[dh // 2 + 1 : dh // 2 + 2]
+            heads[hh] = heads[hh] * fac + got[: dh // 2]
         return unused
 
     slots = jnp.where(z < 2, 1, jnp.where(z < 4, 2, z - 1))
@@ -656,13 +683,12 @@
                 pltpu.VMEM((16, B), bf16),
                 pltpu.VMEM((2, B, B // 2), bf16),
                 pltpu.VMEM((dh, B), f32),
+                pltpu.VMEM((2, dh, B), f32),
                 pltpu.VMEM((8, B), f32),
                 pltpu.VMEM((Z, dh + 8, B), f32),
                 pltpu.VMEM((2 * H, 1, 128), f32),
-                pltpu.VMEM((LAST + 1, T, dh // 2, 128), bf16),
-                pltpu.VMEM((6 * T * H, dh // 2, 128), bf16),
-                pltpu.VMEM((LAST + 1, T, 1, 128), f32),
-                pltpu.VMEM((6 * T * H, 1, 128), f32),
+                pltpu.VMEM((LAST + 1, T, dh // 2 + 8, 128), bf16),
+                pltpu.VMEM((6 * T * H, dh // 2 + 8, 128), bf16),
                 pltpu.VMEM((T * H, dh // 2, 128), f32),
                 dma((T,)),
                 dma((T,)),
@@ -679,8 +705,6 @@
                 dma((1,)),
                 dma(((LAST + 1) * T,)),
                 dma((6 * T * H,)),
-                dma(((LAST + 1) * T,)),
-                dma((6 * T * H,)),
                 dma((7,)),
             ],
             compiler_params=pltpu.CompilerParams(collective_id=0, has_side_effects=True, vmem_limit_bytes=67043328),

time: 71.7 us -> 69.1 us (0.964)
  the two profiles are of different devices: /device:TPU:1 before, /device:TPU:161 now
where the time goes in v5:
time: 69.1 us; the launch traced here: 69 us
  Pallas kernels  67.4 us (98%)
  local copies, waits for them, and re-layouts  1.57 us (2%)
    pallas_call x1, Pallas kernels, local(): pl.pallas_call(functools.partial(layer_kernel, S, T, H, dh), out_shape=ja...  67.4 us
    unnamed x1, local copies, waits for them, and re-layouts  1.57 us

profile of v5, /device:TPU:161, one launch (start us, length us, event | category | flops | bytes accessed | tf_op | source)
XLA Modules:
  0.0 69.0 jit_solution(18168540544025587530)
XLA Ops:
  0.0 67.4 %shard_map.82 = bf16[64,1024]{1,0:T(8,128)(2,1)} custom-call(bf16[64,1024]{1,0:T(8,128)(2,1)} %act_hbm.1, f32[1,1024]{1,0:T(1,128)} %bitcast.2, bf16[1024,128]{1,0:T(8,128)(2,1)} %wq_hbm.1, bf16[1024,128]{1,0:T(8,128)(2,1)} %wk_hbm.1, bf16[1024,128]{1,0:T(8,128)(2,1)} %wv_hbm.1, f32[2]{0:T(128)} %off.1, bf16[128,1024]{1,0:T(8,128)(2,1)} %wo_hbm.1, ...), custom_call_target="tpu_custom_call" | custom-call | tf_op jit(solution)/shard_map/pallas_call | solution.py:664
  67.4 1.6 %copy.10 = bf16[64,1024]{1,0:T(8,128)(2,1)} copy(bf16[64,1024]{1,0:T(8,128)(2,1)} %shard_map.82) | data formatting | bytes 262144

commit v6 on v5

--- a/solution.py
+++ b/solution.py
@@ -41,9 +41,8 @@
     act,
     gain_in,
     gain_out,
-    wq,
-    wk,
-    wv,
+    weights,
+    rows_q,
     xg,
     wg,
     perm,
@@ -130,9 +129,9 @@
     for copy in early:
         copy.start()
     loads = [
-        pltpu.make_async_copy(wk_hbm, wk, load.at[0]),
-        pltpu.make_async_copy(wv_hbm, wv, load.at[1]),
-        pltpu.make_async_copy(wq_hbm, wq, load.at[2]),
+        pltpu.make_async_copy(wk_hbm, weights.at[:, : H * dh], load.at[0]),
+        pltpu.make_async_copy(wv_hbm, weights.at[:, H * dh : 2 * H * dh], load.at[1]),
+        pltpu.make_async_copy(wq_hbm, weights.at[:, 2 * H * dh :], load.at[2]),
         pltpu.make_async_copy(wo_hbm, wrow(t), load.at[3]),
         pltpu.make_async_copy(gain_out_hbm, gain_out, load.at[6]),
     ]
@@ -166,24 +165,30 @@
         offs[H * c + i] = jnp.broadcast_to(off[i] * log2e, (1, 128)).astype(f32)
     mine = offs.at[pl.ds(H * c, H)]
     go(remote(mine, mine, off_send.at[0], off_recv.at[0], (s, partner)))
+    def project(chip):
+        rows_of = pl.ds(pl.multiple_of(chip * 2 * R, 2 * R), 2 * R)
+        rows_q[rows_of] = jnp.dot(xg[rows_of], weights[...], preferred_element_type=f32)
+
+    for copy in loads:
+        copy.wait()
+    x_copy(partner, 0, partner).wait_recv()
+    project(y)
     x_copy(behind * 2 + c, 0, partner).wait_recv()
     go(x_copy(behind * 2 + c, 3, onward * 2 + c))
     go(x_copy(behind * 2 + c, 4, partner))
     x_copy(onward * 2 + c, 0, partner).wait_recv()
     go(x_copy(onward * 2 + c, 5, partner))
+    for chip in (behind, onward):
+        x_copy(chip * 2 + 1 - c, 0, partner).wait_recv()
+        project(chip)
     x_copy(across * 2 + c, 0, partner).wait_recv()
     go(x_copy(across * 2 + c, 6, partner))
-    for copy in loads:
-        copy.wait()
     for e in range(1, Y):
         go(w_copy(wrow(t), t, e, ((y + e) % Y) * 2 + c))
-    x_copy(partner, 0, partner).wait_recv()
-    for e in range(1, Y):
-        x_copy(((y + e) % Y) * 2 + 1 - c, 0, partner).wait_recv()
-
-    rows_all = xg[...]
-    keys = jnp.dot(rows_all, wk[...], preferred_element_type=f32).astype(bf16).astype(f32)
-    values = jnp.dot(rows_all, wv[...], preferred_element_type=f32).astype(bf16).astype(f32)
+    x_copy(across * 2 + 1 - c, 0, partner).wait_recv()
+    project(across)
+    keys = rows_q[:, : H * dh].astype(bf16).astype(f32)
+    values = rows_q[:, H * dh : 2 * H * dh].astype(bf16).astype(f32)
     turned = jnp.concatenate([keys.T, values.T], axis=0).astype(bf16)
     placed = jnp.dot(turned, perm[...], preferred_element_type=f32)
     keys_placed = placed[: H * dh].T
@@ -237,7 +242,7 @@
         def _():
             copy.start()
 
-    queries = jnp.dot(rows_all, wq[...], preferred_element_type=f32) * (dh ** (-0.5) * log2e)
+    queries = rows_q[:, 2 * H * dh :] * (dh ** (-0.5) * log2e)
     q_turned = queries.T.astype(bf16)
     for i in range(H):
         qb[i] = q_turned[i * dh : (i + 1) * dh]
@@ -670,9 +675,8 @@
                 pltpu.VMEM((R, D), bf16),
                 pltpu.VMEM((1, D), f32),
                 pltpu.VMEM((1, D), f32),
-                pltpu.VMEM(wq.shape, bf16),
-                pltpu.VMEM(wk.shape, bf16),
-                pltpu.VMEM(wv.shape, bf16),
+                pltpu.VMEM((D, 3 * H * dh), bf16),
+                pltpu.VMEM((B, 3 * H * dh), f32),
                 pltpu.VMEM((B, D), bf16),
                 pltpu.VMEM((wo.shape[0] * T, D), bf16),
                 pltpu.VMEM((B, B), bf16),

time: 69.1 us -> 67.1 us (0.971)
  the two profiles are of different devices: /device:TPU:161 before, /device:TPU:129 now
where the time goes in v6:
time: 67.1 us; the launch traced here: 66.1 us
  Pallas kernels  64.5 us (96%)
  local copies, waits for them, and re-layouts  1.57 us (2%)
    pallas_call x1, Pallas kernels, local(): pl.pallas_call(functools.partial(layer_kernel, S, T, H, dh), out_shape=ja...  64.5 us
    unnamed x1, local copies, waits for them, and re-layouts  1.57 us

profile of v6, /device:TPU:129, one launch (start us, length us, event | category | flops | bytes accessed | tf_op | source)
XLA Modules:
  0.0 66.1 jit_solution(17857447420060950858)
XLA Ops:
  0.0 64.5 %shard_map.82 = bf16[64,1024]{1,0:T(8,128)(2,1)} custom-call(bf16[64,1024]{1,0:T(8,128)(2,1)} %act_hbm.1, f32[1,1024]{1,0:T(1,128)} %bitcast.2, bf16[1024,128]{1,0:T(8,128)(2,1)} %wq_hbm.1, bf16[1024,128]{1,0:T(8,128)(2,1)} %wk_hbm.1, bf16[1024,128]{1,0:T(8,128)(2,1)} %wv_hbm.1, f32[2]{0:T(128)} %off.1, bf16[128,1024]{1,0:T(8,128)(2,1)} %wo_hbm.1, ...), custom_call_target="tpu_custom_call" | custom-call | tf_op jit(solution)/shard_map/pallas_call | solution.py:669
  64.5 1.6 %copy.10 = bf16[64,1024]{1,0:T(8,128)(2,1)} copy(bf16[64,1024]{1,0:T(8,128)(2,1)} %shard_map.82) | data formatting | bytes 262144

commit v7 on v6

--- a/solution.py
+++ b/solution.py
@@ -116,8 +116,20 @@
     def wrow(index):
         return wg.at[pl.ds(pl.multiple_of(index * rows, rows), rows)]
 
-    def x_copy(index, slot, dev):
-        return remote(xrow(index), xrow(index), x_send.at[slot], x_recv.at[index], (s, dev))
+    def x_part(index, slot, dev, part):
+        half = xg.at[pl.ds(pl.multiple_of(index * R + part * (R // 2), R // 2), R // 2)]
+        return remote(half, half, x_send.at[2 * slot + part], x_recv.at[2 * index + part], (s, dev))
+
+    def x_sends(index, *targets):
+        for part in range(2):
+            for slot, dev in targets:
+                go(x_part(index, slot, dev, part))
+
+    def x_take(index, *targets):
+        for part in range(2):
+            x_part(index, 0, partner, part).wait_recv()
+            for slot, dev in targets:
+                go(x_part(index, slot, dev, part))
 
     def w_copy(src, index, slot, dev):
         return remote(src, wrow(index), w_send.at[slot], w_recv.at[index], (s, dev))
@@ -154,9 +166,7 @@
     onward = (y + 1 + (Y - 2) * c) % Y
     behind = (y + Y - 1 - (Y - 2) * c) % Y
     across = (y + 2) % Y
-    go(x_copy(t, 1, onward * 2 + c))
-    go(x_copy(t, 2, behind * 2 + c))
-    go(x_copy(t, 0, partner))
+    x_sends(t, (1, onward * 2 + c), (2, behind * 2 + c), (0, partner))
 
     token = lax.broadcasted_iota(jnp.int32, (B, B), 0)
     place = lax.broadcasted_iota(jnp.int32, (B, B), 1)
@@ -171,21 +181,17 @@
 
     for copy in loads:
         copy.wait()
-    x_copy(partner, 0, partner).wait_recv()
+    x_take(partner)
     project(y)
-    x_copy(behind * 2 + c, 0, partner).wait_recv()
-    go(x_copy(behind * 2 + c, 3, onward * 2 + c))
-    go(x_copy(behind * 2 + c, 4, partner))
-    x_copy(onward * 2 + c, 0, partner).wait_recv()
-    go(x_copy(onward * 2 + c, 5, partner))
+    x_take(behind * 2 + c, (3, onward * 2 + c), (4, partner))
+    x_take(onward * 2 + c, (5, partner))
     for chip in (behind, onward):
-        x_copy(chip * 2 + 1 - c, 0, partner).wait_recv()
+        x_take(chip * 2 + 1 - c)
         project(chip)
-    x_copy(across * 2 + c, 0, partner).wait_recv()
-    go(x_copy(across * 2 + c, 6, partner))
+    x_take(across * 2 + c, (6, partner))
     for e in range(1, Y):
         go(w_copy(wrow(t), t, e, ((y + e) % Y) * 2 + c))
-    x_copy(across * 2 + 1 - c, 0, partner).wait_recv()
+    x_take(across * 2 + 1 - c)
     project(across)
     keys = rows_q[:, : H * dh].astype(bf16).astype(f32)
     values = rows_q[:, H * dh : 2 * H * dh].astype(bf16).astype(f32)
@@ -694,8 +700,8 @@
                 pltpu.VMEM((LAST + 1, T, dh // 2 + 8, 128), bf16),
                 pltpu.VMEM((6 * T * H, dh // 2 + 8, 128), bf16),
                 pltpu.VMEM((T * H, dh // 2, 128), f32),
-                dma((T,)),
-                dma((T,)),
+                dma((2 * T,)),
+                dma((2 * T,)),
                 dma((T,)),
                 dma((T,)),
                 dma((16,)),

time: 67.1 us -> 66.2 us (0.987); the launches traced: 66.1 us -> 66.1 us
  no operation moved by 1% of the time
where the time goes in v7:
time: 66.2 us; the launch traced here: 66.1 us
  Pallas kernels  64.5 us (97%)
  local copies, waits for them, and re-layouts  1.57 us (2%)
    pallas_call x1, Pallas kernels, local(): pl.pallas_call(functools.partial(layer_kernel, S, T, H, dh), out_shape=ja...  64.5 us
    unnamed x1, local copies, waits for them, and re-layouts  1.57 us

profile of v7, /device:TPU:129, one launch (start us, length us, event | category | flops | bytes accessed | tf_op | source)
XLA Modules:
  0.0 66.1 jit_solution(4278747656184758179)
XLA Ops:
  0.0 64.5 %shard_map.82 = bf16[64,1024]{1,0:T(8,128)(2,1)} custom-call(bf16[64,1024]{1,0:T(8,128)(2,1)} %act_hbm.1, f32[1,1024]{1,0:T(1,128)} %bitcast.2, bf16[1024,128]{1,0:T(8,128)(2,1)} %wq_hbm.1, bf16[1024,128]{1,0:T(8,128)(2,1)} %wk_hbm.1, bf16[1024,128]{1,0:T(8,128)(2,1)} %wv_hbm.1, f32[2]{0:T(128)} %off.1, bf16[128,1024]{1,0:T(8,128)(2,1)} %wo_hbm.1, ...), custom_call_target="tpu_custom_call" | custom-call | tf_op jit(solution)/shard_map/pallas_call | solution.py:675
  64.5 1.6 %copy.10 = bf16[64,1024]{1,0:T(8,128)(2,1)} copy(bf16[64,1024]{1,0:T(8,128)(2,1)} %shard_map.82) | data formatting | bytes 262144

commit v8 on v7

--- a/solution.py
+++ b/solution.py
@@ -16,7 +16,7 @@
 ZMAX = 63.0
 LAST = 11
 FIRST = 5
-SELF_TURN = 9
+SELF_TURN = 7
 
 
 def scaled_rows(widened, row_gain):

time: 66.2 us -> 65.9 us (level)
  no operation moved by 1% of the time
where the time goes in v8:
time: 65.9 us; the launch traced here: 65.7 us
  Pallas kernels  64.2 us (97%)
  local copies, waits for them, and re-layouts  1.57 us (2%)
    pallas_call x1, Pallas kernels, local(): pl.pallas_call(functools.partial(layer_kernel, S, T, H, dh), out_shape=ja...  64.2 us
    unnamed x1, local copies, waits for them, and re-layouts  1.57 us

profile of v8, /device:TPU:129, one launch (start us, length us, event | category | flops | bytes accessed | tf_op | source)
XLA Modules:
  0.0 65.7 jit_solution(6018762731015407834)
XLA Ops:
  0.0 64.2 %shard_map.82 = bf16[64,1024]{1,0:T(8,128)(2,1)} custom-call(bf16[64,1024]{1,0:T(8,128)(2,1)} %act_hbm.1, f32[1,1024]{1,0:T(1,128)} %bitcast.2, bf16[1024,128]{1,0:T(8,128)(2,1)} %wq_hbm.1, bf16[1024,128]{1,0:T(8,128)(2,1)} %wk_hbm.1, bf16[1024,128]{1,0:T(8,128)(2,1)} %wv_hbm.1, f32[2]{0:T(128)} %off.1, bf16[128,1024]{1,0:T(8,128)(2,1)} %wo_hbm.1, ...), custom_call_target="tpu_custom_call" | custom-call | tf_op jit(solution)/shard_map/pallas_call | solution.py:675
  64.2 1.6 %copy.10 = bf16[64,1024]{1,0:T(8,128)(2,1)} copy(bf16[64,1024]{1,0:T(8,128)(2,1)} %shard_map.82) | data formatting | bytes 262144

commit v9 on v8

--- a/solution.py
+++ b/solution.py
@@ -15,8 +15,8 @@
 XS = 4
 ZMAX = 63.0
 LAST = 11
-FIRST = 5
-SELF_TURN = 7
+FIRST = 6
+SELF_TURN = 8
 
 
 def scaled_rows(widened, row_gain):
@@ -506,7 +506,7 @@
 
         @pl.when(turn == FIRST)
         def _():
-            for step in (0, 1, Z - 1):
+            for step in (0, 1):
                 close = (z + step) % Z
 
                 @pl.when(close >= Z - 1 - 2 * g)

time: 65.9 us -> 65.8 us (level)
  no operation moved by 1% of the time
where the time goes in v9:
time: 65.8 us; the launch traced here: 65.7 us
  Pallas kernels  64.2 us (98%)
  local copies, waits for them, and re-layouts  1.57 us (2%)
    pallas_call x1, Pallas kernels, local(): pl.pallas_call(functools.partial(layer_kernel, S, T, H, dh), out_shape=ja...  64.2 us
    unnamed x1, local copies, waits for them, and re-layouts  1.57 us

profile of v9, /device:TPU:129, one launch (start us, length us, event | category | flops | bytes accessed | tf_op | source)
XLA Modules:
  0.0 65.7 jit_solution(16376046269078217549)
XLA Ops:
  0.0 64.2 %shard_map.82 = bf16[64,1024]{1,0:T(8,128)(2,1)} custom-call(bf16[64,1024]{1,0:T(8,128)(2,1)} %act_hbm.1, f32[1,1024]{1,0:T(1,128)} %bitcast.2, bf16[1024,128]{1,0:T(8,128)(2,1)} %wq_hbm.1, bf16[1024,128]{1,0:T(8,128)(2,1)} %wk_hbm.1, bf16[1024,128]{1,0:T(8,128)(2,1)} %wv_hbm.1, f32[2]{0:T(128)} %off.1, bf16[128,1024]{1,0:T(8,128)(2,1)} %wo_hbm.1, ...), custom_call_target="tpu_custom_call" | custom-call | tf_op jit(solution)/shard_map/pallas_call | solution.py:675
  64.2 1.6 %copy.10 = bf16[64,1024]{1,0:T(8,128)(2,1)} copy(bf16[64,1024]{1,0:T(8,128)(2,1)} %shard_map.82) | data formatting | bytes 262144
